TPU v7x, 32 devices: a whole 2x2x4 slice. The times are simulated.
32 devices in a mesh: sp: 8 (over z, x), tp: 4 (over y, core).
Axes of the slice: x: 2, y: 2, z: 4, core: 2. Of those that a mesh axis runs over, the one named last changes fastest.
Arguments:
- tokens: bfloat16 [2, 1536, 4096], P(None, 'sp', 'tp'), may hold values from -12 to 12
- query_weight: bfloat16 [4096, 2048], P(None, 'tp'), may hold values from -0.09375 to 0.09375
- key_weight: bfloat16 [4096, 2048], P(None, 'tp'), may hold values from -0.09375 to 0.09375
- value_weight: bfloat16 [4096, 2048], P(None, 'tp'), may hold values from -0.09375 to 0.09375
- gate_weight: bfloat16 [4096, 2048], P(None, 'tp'), may hold values from -0.09375 to 0.09375
- beta_weight: bfloat16 [4096, 16], P(None, 'tp'), may hold values from -0.09375 to 0.09375
- decay_weight: bfloat16 [4096, 16], P(None, 'tp'), may hold values from -0.09375 to 0.09375
- beta_bias: float32 [16], P('tp'), may hold values from -6 to -3
- rate_log: float32 [16], P('tp'), may hold values from -12 to -2.5
- out_gain: float32 [128], replicated, may hold values from 0.1 to 1.9
- new_query: bfloat16 [2, 16, 128], P(None, 'tp'), may hold values from -6 to 6
- new_key: bfloat16 [2, 16, 128], P(None, 'tp'), may hold values from -6 to 6
- new_value: bfloat16 [2, 16, 128], P(None, 'tp'), may hold values from -6 to 6
- new_beta: float32 [2, 16], P(None, 'tp'), may hold values from 0.1 to 0.9
- new_decay: float32 [2, 16], P(None, 'tp'), may hold values from 0.3 to 1
Outputs:
- mixed_out: bfloat16 [2, 1536, 2048], P(None, 'sp', 'tp')
- cache: bfloat16 [2, 16, 128, 128], P(None, 'tp', 'sp')
- first_out: float32 [2, 2048], P(None, 'tp')
All inputs are finite; a program needn't handle non-finite values.
Results may differ from a plain program's by a relative error of at most 0.0073.
Values may be sent and summed in bfloat16 or wider, within the bound.
A program may use at most 64 MiB of HBM per device.

v0:
```python
import jax
import jax.numpy as jnp
from jax import lax
from jax.sharding import PartitionSpec as P

BLOCK = 64


unit_floor = 1.0
norm_floor = 0.001
highest = lax.Precision.HIGHEST


def shifted(value, axis, steps):
    count = lax.axis_size(axis)
    first, last = (max(0, -steps), min(count, count - steps))
    return lax.ppermute(value, axis, [(source, source + steps) for source in range(first, last)])


def matmul(form, left, right):
    return jnp.einsum(form, left, right, precision=highest)


def unit_rows(values):
    return values * lax.rsqrt(jnp.sum(values * values, axis=-1, keepdims=True) + unit_floor)


def head_norm(values, out_gain):
    return (
        values
        * lax.rsqrt(jnp.mean(values * values, axis=-1, keepdims=True) + norm_floor)
        * out_gain
    )


def stored(values):
    return lax.optimization_barrier(values.astype(jnp.bfloat16)).astype(jnp.float32)


def unit_lower_inverse(lower_part):
    extent = lower_part.shape[-1]
    nilpotent = -lower_part
    inverse = jnp.eye(extent, dtype=jnp.float32) + nilpotent
    for _ in range(extent.bit_length() - 2):
        nilpotent = matmul("...ij,...jk->...ik", nilpotent, nilpotent)
        inverse = inverse + matmul("...ij,...jk->...ik", nilpotent, inverse)
    return inverse


def prepare(
    query_rows,
    key_rows,
    value_rows,
    beta_in,
    decay_in,
    beta_bias,
    rate_log,
    seq_count,
    length,
    head_count,
):
    extent = query_rows.shape[-1] // head_count
    blocks = length // BLOCK

    def by_head(values):
        shaped = values.reshape(seq_count, blocks, BLOCK, head_count, extent)
        return shaped.transpose(0, 3, 1, 2, 4).reshape(
            seq_count * head_count, blocks, BLOCK, extent
        )

    def by_scalar(values):
        shaped = values.reshape(seq_count, blocks, BLOCK, head_count)
        return shaped.transpose(0, 3, 1, 2).reshape(seq_count * head_count, blocks, BLOCK)

    queries = unit_rows(by_head(query_rows))
    key_unit = unit_rows(by_head(key_rows))
    values = by_head(value_rows)
    strength = by_scalar(jax.nn.sigmoid(beta_in + beta_bias))
    decays = by_scalar(-jnp.exp(rate_log) * jax.nn.softplus(decay_in))
    return (queries, key_unit, values, strength, decays)


def block_terms(queries, key_unit, values, strength, decays):
    extent = decays.shape[-1]
    cumulative = jnp.cumsum(decays, axis=-1)
    causal = jnp.tril(jnp.ones((extent, extent), bool))
    strict = jnp.tril(jnp.ones((extent, extent), bool), -1)
    spread = cumulative[..., :, None] - cumulative[..., None, :]
    weights = jnp.where(causal, jnp.exp(jnp.where(causal, spread, 0.0)), 0.0)
    key_beta = key_unit * strength[..., None]
    lower_part = jnp.where(strict, matmul("...td,...sd->...ts", key_beta, key_unit) * weights, 0.0)
    inverse = unit_lower_inverse(lower_part)
    update = matmul("...ts,...se->...te", inverse, values * strength[..., None])
    carry_w = matmul("...ts,...sd->...td", inverse, key_beta * jnp.exp(cumulative)[..., None])
    scores = matmul("...td,...sd->...ts", queries, key_unit) * weights
    query_decay = queries * jnp.exp(cumulative)[..., None]
    last_log = cumulative[..., -1]
    key_decay = key_unit * jnp.exp(last_log[..., None] - cumulative)[..., None]
    return (update, carry_w, query_decay, scores, key_decay, last_log)


def finish_read(recall, retrieve, query_unit, key_unit, new_value, new_beta, new_decay, out_gain):
    seq_count, head_count, extent = recall.shape
    intersect = jnp.sum(key_unit * query_unit, axis=-1)
    fresh_values = new_value.astype(jnp.float32) - new_decay[..., None] * retrieve
    read_heads = new_decay[..., None] * recall + (new_beta * intersect)[..., None] * fresh_values
    return head_norm(read_heads, out_gain).reshape(seq_count, head_count * extent)


def project_rows(shard_rows, weights):
    row_count = shard_rows.shape[-1]
    flat_rows = shard_rows.reshape(-1, row_count)
    return tuple(
        (jnp.dot(flat_rows, weight, preferred_element_type=jnp.float32) for weight in weights)
    )


def shards(
    tokens,
    query_weight,
    key_weight,
    value_weight,
    gate_weight,
    beta_weight,
    decay_weight,
    beta_bias,
    rate_log,
    out_gain,
    new_query,
    new_key,
    new_value,
    new_beta,
    new_decay,
):
    seq_count, span_len, _ = tokens.shape
    head_count = rate_log.shape[0]
    weights = (query_weight, key_weight, value_weight, gate_weight, beta_weight, decay_weight)
    totals = project_rows(lax.all_gather(tokens, "tp", axis=2, tiled=True), weights)
    query_rows = stored(totals[0])
    key_rows = stored(totals[1])
    value_rows = stored(totals[2])
    gate_rows = stored(totals[3])
    prepared = prepare(
        query_rows,
        key_rows,
        value_rows,
        totals[4],
        totals[5],
        beta_bias,
        rate_log,
        seq_count,
        span_len,
        head_count,
    )
    block_data = block_terms(*prepared)
    batch_size = block_data[0].shape[0]
    extent = block_data[0].shape[-1]
    identity = jnp.broadcast_to(jnp.eye(extent, dtype=jnp.float32), (batch_size, extent, extent))

    def advance(carried, inputs):
        state_now, reach_map = carried
        u_block, w_block, qg_block, score_block, kd_block, gl_block = inputs
        fresh_values = u_block - matmul("btd,bde->bte", w_block, state_now)
        block_out = matmul("btd,bde->bte", qg_block, state_now) + matmul(
            "bts,bse->bte", score_block, fresh_values
        )
        reach_rows = qg_block - matmul("bts,bsd->btd", score_block, w_block)
        factor = jnp.exp(gl_block)[:, None, None]
        transit = factor * identity - matmul("bsd,bse->bde", kd_block, w_block)
        state_next = state_now * factor + matmul("bsd,bse->bde", kd_block, fresh_values)
        map_next = matmul("bde,bef->bdf", transit, reach_map)
        return ((state_next, map_next), (block_out, matmul("btd,bde->bte", reach_rows, reach_map)))

    inputs = tuple((jnp.moveaxis(member, 1, 0) for member in block_data))
    start_state = jnp.zeros((batch_size, extent, extent), jnp.float32)
    (local_state, local_map), (local_out, reach_all) = lax.scan(
        advance, (start_state, identity), inputs
    )

    def turn(turn_index, incoming):
        outgoing = matmul("bde,bef->bdf", local_map, incoming) + local_state
        return shifted(outgoing, "sp", 1)

    incoming = lax.fori_loop(0, lax.axis_size("sp") - 1, turn, jnp.zeros_like(local_state))
    block_total = local_out + matmul("nbtd,bde->nbte", reach_all, incoming)
    blocks = span_len // BLOCK
    heads_out = block_total.reshape(blocks, seq_count, head_count, BLOCK, extent).transpose(
        1, 0, 3, 2, 4
    )
    heads_out = heads_out.reshape(seq_count, span_len, head_count, extent)
    gate_values = gate_rows.reshape(seq_count, span_len, head_count, extent)
    mixed_out = (head_norm(heads_out, out_gain) * jax.nn.silu(gate_values)).astype(jnp.bfloat16)
    mixed_out = mixed_out.reshape(seq_count, span_len, head_count * extent)
    final_state = matmul("bde,bef->bdf", local_map, incoming) + local_state
    final_cast = final_state.reshape(seq_count, head_count, extent, extent).astype(jnp.bfloat16)
    row_count = extent // lax.axis_size("sp")
    row_start = lax.axis_index("sp") * row_count
    query_unit = unit_rows(new_query.astype(jnp.float32))
    key_unit = unit_rows(new_key.astype(jnp.float32))
    is_last = lax.axis_index("sp") == lax.axis_size("sp") - 1
    own_term = jnp.where(is_last, final_cast.astype(jnp.float32), 0.0)
    cache_rows = lax.psum_scatter(
        own_term.astype(jnp.bfloat16), "sp", scatter_dimension=2, tiled=True
    )
    memory = lax.optimization_barrier(cache_rows).astype(jnp.float32)
    query_part = lax.dynamic_slice_in_dim(query_unit, row_start, row_count, 2)
    key_part = lax.dynamic_slice_in_dim(key_unit, row_start, row_count, 2)
    recall, retrieve = lax.psum(
        (matmul("shde,shd->she", memory, query_part), matmul("shde,shd->she", memory, key_part)),
        "sp",
    )
    first_out = finish_read(
        recall, retrieve, query_unit, key_unit, new_value, new_beta, new_decay, out_gain
    )
    return (mixed_out, cache_rows, first_out)


def solution(mesh):
    placed = (
        P(None, "sp", "tp"),
        P(None, "tp"),
        P(None, "tp"),
        P(None, "tp"),
        P(None, "tp"),
        P(None, "tp"),
        P(None, "tp"),
        P("tp"),
        P("tp"),
        P(),
        P(None, "tp", None),
        P(None, "tp", None),
        P(None, "tp", None),
        P(None, "tp"),
        P(None, "tp"),
    )
    return jax.shard_map(
        shards,
        mesh=mesh,
        in_specs=placed,
        out_specs=(P(None, "sp", "tp"), P(None, "tp", "sp", None), P(None, "tp")),
        check_vma=False,
    )
```

profile of v0, /device:TPU:0, one launch (start us, length us, event | category | flops | bytes accessed | tf_op | source)
XLA Modules:
  0.0 305.5 jit_solution(13586617555090404799)
XLA Ops:
  13.8 27.1 %all-gather.2.cloned.1.call-done = bf16[2,192,4096]{2,1,0:T(8,128)(2,1)} async-done(((bf16[2,192,1024]{2,1,0:T(8,128)(2,1)}), bf16[2,192,4096]{2,1,0:T(8,128)(2,1)}) %all-gather.2.cloned.1.call-update) | async-done | bytes 3145744 | tf_op jit(solution)/shard_map/all_gather | solution.py:138
  40.9 2.8 fusion.66
  44.7 5.8 %convolution_convert_fusion = bf16[384,512]{1,0:T(8,128)(2,1)} fusion(bf16[384,4096]{1,0:T(8,128)(2,1)} %bitcast.200, bf16[4096,512]{1,0:T(8,128)(2,1)} %param.23), kind=kOutput, calls=%fused_computation.59 | convolution fusion | flops 1610809344 | bytes 7733248 | tf_op jit(solution)/shard_map/dot_general | solution.py:114
  53.4 2.8 fusion.49
  56.3 4.9 %convolution_convert_fusion.3 = bf16[384,512]{1,0:T(8,128)(2,1)S(1)} fusion(bf16[384,4096]{1,0:T(8,128)(2,1)} %bitcast.202, bf16[4096,512]{1,0:T(8,128)(2,1)} %param.21), kind=kOutput, calls=%fused_computation.62 | convolution fusion | flops 1610809344 | bytes 7733248 | tf_op jit(solution)/shard_map/dot_general | solution.py:114
  62.2 4.9 %convolution_convert_fusion.2 = bf16[384,512]{1,0:T(8,128)(2,1)S(1)} fusion(bf16[384,4096]{1,0:T(8,128)(2,1)} %bitcast.203, bf16[4096,512]{1,0:T(8,128)(2,1)} %param.22), kind=kOutput, calls=%fused_computation.61 | convolution fusion | flops 1610809344 | bytes 7733248 | tf_op jit(solution)/shard_map/dot_general | solution.py:114
  85.0 23.5 %while.28 = (s32[]{:T(128)}, f32[8,128,128]{2,1,0:T(8,128)S(1)}, f32[8,128,128]{2,1,0:T(8,128)S(1)}, f32[3,8,64,128]{3,2,0,1:T(8,128)}, f32[3,8,64,128]{3,2,0,1:...) while((s32[]{:T(128)}, f32[8,128,128]{2,1,0:T(8,128)S(1)}, ...), condition=%wide.region_4.5_spmd.clone, body=%wide.region_3.4_spmd.clone.sunk | while | flops 806420480 | bytes 12392708 | solution.py:176
  108.5 101.1 %while.27 = (s32[]{:T(128)}, f32[8,128,128]{2,1,0:T(8,128)S(1)}, f32[8,128,128]{2,1,0:T(8,128)S(1)}, f32[8,128,128]{2,1,0:T(8,128)S(1)}, s32[]{:T(128)}) while((s32[]{:T(128)}, f32[8,128,128]{2,1,0:T(8,128)S(1)}, f32[8,128,128]{2,1,0:T(8,128)S(1)}, f32[8,128,128]{2,1,0:T(8,128)S(1)}, s32[]{:T(128)}) %tuple.60), condition=%wide.region_6.7_spmd, body=%wide.region_5.6_spmd.sunk | while | flops 201457664 | bytes 4194405 | solution.py:184
  109.2 3.4 %collective-permute-start = (f32[8,128,128]{2,1,0:T(8,128)S(1)}, f32[8,128,128]{2,1,0:T(8,128)S(1)}, u32[]{:S(2)}, u32[]{:S(2)}) collective-permute-start(f32[8,128,128]{2,1,0:T(8,128)S(1)} %convolution_add_fusion.12), channel_id=1, source_target_pairs={{0,4},{4,8},{8,12},{12,16},{16,20},{20,24},{24,28},{1,5},{5,9},{9,... | collective-permute-start | bytes 1572872 | tf_op jit(solution)/shard_map/while/body/eval_jaxpr/ppermute | solution.py:17
  112.6 11.5 %collective-permute-done = f32[8,128,128]{2,1,0:T(8,128)S(1)} collective-permute-done((f32[8,128,128]{2,1,0:T(8,128)S(1)}, f32[8,128,128]{2,1,0:T(8,128)S(1)}, u32[]{:S(2)}, u32[]{:S(2)}) %collective-permute-start) | collective-permute-done | bytes 524320 | tf_op jit(solution)/shard_map/while/body/eval_jaxpr/ppermute | solution.py:17
  124.8 4.4 %collective-permute-start = (f32[8,128,128]{2,1,0:T(8,128)S(1)}, f32[8,128,128]{2,1,0:T(8,128)S(1)}, u32[]{:S(2)}, u32[]{:S(2)}) collective-permute-start(f32[8,128,128]{2,1,0:T(8,128)S(1)} %convolution_add_fusion.12), channel_id=1, source_target_pairs={{0,4},{4,8},{8,12},{12,16},{16,20},{20,24},{24,28},{1,5},{5,9},{9,... | collective-permute-start | bytes 1572872 | tf_op jit(solution)/shard_map/while/body/eval_jaxpr/ppermute | solution.py:17
  129.2 10.7 %collective-permute-done = f32[8,128,128]{2,1,0:T(8,128)S(1)} collective-permute-done((f32[8,128,128]{2,1,0:T(8,128)S(1)}, f32[8,128,128]{2,1,0:T(8,128)S(1)}, u32[]{:S(2)}, u32[]{:S(2)}) %collective-permute-start) | collective-permute-done | bytes 524320 | tf_op jit(solution)/shard_map/while/body/eval_jaxpr/ppermute | solution.py:17
  140.6 4.4 %collective-permute-start = (f32[8,128,128]{2,1,0:T(8,128)S(1)}, f32[8,128,128]{2,1,0:T(8,128)S(1)}, u32[]{:S(2)}, u32[]{:S(2)}) collective-permute-start(f32[8,128,128]{2,1,0:T(8,128)S(1)} %convolution_add_fusion.12), channel_id=1, source_target_pairs={{0,4},{4,8},{8,12},{12,16},{16,20},{20,24},{24,28},{1,5},{5,9},{9,... | collective-permute-start | bytes 1572872 | tf_op jit(solution)/shard_map/while/body/eval_jaxpr/ppermute | solution.py:17
  145.0 9.8 %collective-permute-done = f32[8,128,128]{2,1,0:T(8,128)S(1)} collective-permute-done((f32[8,128,128]{2,1,0:T(8,128)S(1)}, f32[8,128,128]{2,1,0:T(8,128)S(1)}, u32[]{:S(2)}, u32[]{:S(2)}) %collective-permute-start) | collective-permute-done | bytes 524320 | tf_op jit(solution)/shard_map/while/body/eval_jaxpr/ppermute | solution.py:17
  155.5 5.2 %collective-permute-start = (f32[8,128,128]{2,1,0:T(8,128)S(1)}, f32[8,128,128]{2,1,0:T(8,128)S(1)}, u32[]{:S(2)}, u32[]{:S(2)}) collective-permute-start(f32[8,128,128]{2,1,0:T(8,128)S(1)} %convolution_add_fusion.12), channel_id=1, source_target_pairs={{0,4},{4,8},{8,12},{12,16},{16,20},{20,24},{24,28},{1,5},{5,9},{9,... | collective-permute-start | bytes 1572872 | tf_op jit(solution)/shard_map/while/body/eval_jaxpr/ppermute | solution.py:17
  160.7 9.0 %collective-permute-done = f32[8,128,128]{2,1,0:T(8,128)S(1)} collective-permute-done((f32[8,128,128]{2,1,0:T(8,128)S(1)}, f32[8,128,128]{2,1,0:T(8,128)S(1)}, u32[]{:S(2)}, u32[]{:S(2)}) %collective-permute-start) | collective-permute-done | bytes 524320 | tf_op jit(solution)/shard_map/while/body/eval_jaxpr/ppermute | solution.py:17
  170.3 5.3 %collective-permute-start = (f32[8,128,128]{2,1,0:T(8,128)S(1)}, f32[8,128,128]{2,1,0:T(8,128)S(1)}, u32[]{:S(2)}, u32[]{:S(2)}) collective-permute-start(f32[8,128,128]{2,1,0:T(8,128)S(1)} %convolution_add_fusion.12), channel_id=1, source_target_pairs={{0,4},{4,8},{8,12},{12,16},{16,20},{20,24},{24,28},{1,5},{5,9},{9,... | collective-permute-start | bytes 1572872 | tf_op jit(solution)/shard_map/while/body/eval_jaxpr/ppermute | solution.py:17
  175.7 8.1 %collective-permute-done = f32[8,128,128]{2,1,0:T(8,128)S(1)} collective-permute-done((f32[8,128,128]{2,1,0:T(8,128)S(1)}, f32[8,128,128]{2,1,0:T(8,128)S(1)}, u32[]{:S(2)}, u32[]{:S(2)}) %collective-permute-start) | collective-permute-done | bytes 524320 | tf_op jit(solution)/shard_map/while/body/eval_jaxpr/ppermute | solution.py:17
  184.4 5.3 %collective-permute-start = (f32[8,128,128]{2,1,0:T(8,128)S(1)}, f32[8,128,128]{2,1,0:T(8,128)S(1)}, u32[]{:S(2)}, u32[]{:S(2)}) collective-permute-start(f32[8,128,128]{2,1,0:T(8,128)S(1)} %convolution_add_fusion.12), channel_id=1, source_target_pairs={{0,4},{4,8},{8,12},{12,16},{16,20},{20,24},{24,28},{1,5},{5,9},{9,... | collective-permute-start | bytes 1572872 | tf_op jit(solution)/shard_map/while/body/eval_jaxpr/ppermute | solution.py:17
  189.8 7.3 %collective-permute-done = f32[8,128,128]{2,1,0:T(8,128)S(1)} collective-permute-done((f32[8,128,128]{2,1,0:T(8,128)S(1)}, f32[8,128,128]{2,1,0:T(8,128)S(1)}, u32[]{:S(2)}, u32[]{:S(2)}) %collective-permute-start) | collective-permute-done | bytes 524320 | tf_op jit(solution)/shard_map/while/body/eval_jaxpr/ppermute | solution.py:17
  197.7 5.3 %collective-permute-start = (f32[8,128,128]{2,1,0:T(8,128)S(1)}, f32[8,128,128]{2,1,0:T(8,128)S(1)}, u32[]{:S(2)}, u32[]{:S(2)}) collective-permute-start(f32[8,128,128]{2,1,0:T(8,128)S(1)} %convolution_add_fusion.12), channel_id=1, source_target_pairs={{0,4},{4,8},{8,12},{12,16},{16,20},{20,24},{24,28},{1,5},{5,9},{9,... | collective-permute-start | bytes 1572872 | tf_op jit(solution)/shard_map/while/body/eval_jaxpr/ppermute | solution.py:17
  203.0 6.6 %collective-permute-done = f32[8,128,128]{2,1,0:T(8,128)S(1)} collective-permute-done((f32[8,128,128]{2,1,0:T(8,128)S(1)}, f32[8,128,128]{2,1,0:T(8,128)S(1)}, u32[]{:S(2)}, u32[]{:S(2)}) %collective-permute-start) | collective-permute-done | bytes 524320 | tf_op jit(solution)/shard_map/while/body/eval_jaxpr/ppermute | solution.py:17
  216.2 60.0 %reduce-scatter.2.cloned.1.call-done = bf16[2,4,16,128]{3,2,1,0:T(8,128)(2,1)} async-done(((bf16[2,4,128,128]{3,2,1,0:T(8,128)(2,1)}), bf16[2,4,16,128]{3,2,1,0:T(8,128)(2,1)}) %reduce-scatter.2.cloned.1.call-update) | async-done | bytes 32784 | tf_op jit(solution)/shard_map/reduce_scatter | solution.py:202
  278.0 19.8 %all-reduce = (f32[2,4,128]{2,1,0:T(4,128)S(1)}, f32[2,4,128]{2,1,0:T(4,128)S(1)}) all-reduce(f32[2,4,128]{2,1,0:T(4,128)S(1)} %bitcast.225, f32[2,4,128]{2,1,0:T(4,128)S(1)} %bitcast.226), channel_id=1, replica_groups=mesh['sp'=8,'tp'=4] {'sp'}, use_global_device_ids=true, to_apply=%region_13.14 | all-reduce | flops 2048 | bytes 16384 | tf_op jit(solution)/shard_map/psum | solution.py:208
  (145 shorter events, 65.9 us)
Async XLA Ops:
  7.2 33.7 %copy-start = (bf16[4096,4]{0,1:T(4,128)(2,1)S(1)}, bf16[4096,4]{0,1:T(4,128)(2,1)}, u32[]{:S(2)}) copy-start(bf16[4096,4]{0,1:T(4,128)(2,1)} %param.25) | copy-start | bytes 98308
  7.2 33.7 %all-gather.2.cloned.1.call-start = ((), (), s32[]{:S(2)}) async-start(), calls=%async_computation.1 | async-start | bytes 3932160 | tf_op jit(solution)/shard_map/all_gather | solution.py:138
  7.9 268.2 %reduce-scatter.2.cloned.1.call-start = ((), (), s32[]{:S(2)}) async-start(), calls=%async_computation.2 | async-start | bytes 294912 | tf_op jit(solution)/shard_map/reduce_scatter | solution.py:202
  44.6 5.9 %copy-start.1 = (bf16[2,192,4096]{2,1,0:T(8,128)(2,1)S(1)}, bf16[2,192,4096]{2,1,0:T(8,128)(2,1)}, u32[]{:S(2)}) copy-start(bf16[2,192,4096]{2,1,0:T(8,128)(2,1)} %all-gather.2.cloned.1.call-done) | copy-start | bytes 9437188
  44.7 5.9 %copy-start.13 = (bf16[4096,512]{1,0:T(8,128)(2,1)S(1)}, bf16[4096,512]{1,0:T(8,128)(2,1)}, u32[]{:S(2)}) copy-start(bf16[4096,512]{1,0:T(8,128)(2,1)} %param.20) | copy-start | bytes 12582916
  52.4 1.0 copy-start.5
  67.5 1.5 copy-start.6
  85.0 3.3 %copy-start.2 = (f32[3,8,64,64]{3,2,0,1:T(8,128)S(1)}, f32[3,8,64,64]{3,2,0,1:T(8,128)}, u32[]{:S(2)}) copy-start(f32[3,8,64,64]{3,2,0,1:T(8,128)} %get-tuple-element.397) | copy-start | bytes 1179652 | tf_op jit(solution)/shard_map/while
  92.8 3.3 %copy-start.2 = (f32[3,8,64,64]{3,2,0,1:T(8,128)S(1)}, f32[3,8,64,64]{3,2,0,1:T(8,128)}, u32[]{:S(2)}) copy-start(f32[3,8,64,64]{3,2,0,1:T(8,128)} %get-tuple-element.397) | copy-start | bytes 1179652 | tf_op jit(solution)/shard_map/while
  100.7 3.3 %copy-start.2 = (f32[3,8,64,64]{3,2,0,1:T(8,128)S(1)}, f32[3,8,64,64]{3,2,0,1:T(8,128)}, u32[]{:S(2)}) copy-start(f32[3,8,64,64]{3,2,0,1:T(8,128)} %get-tuple-element.397) | copy-start | bytes 1179652 | tf_op jit(solution)/shard_map/while
  108.5 102.5 %copy-start.3 = (f32[3,8,64,128]{3,2,0,1:T(8,128)S(1)}, f32[3,8,64,128]{3,2,0,1:T(8,128)}, u32[]{:S(2)}) copy-start(f32[3,8,64,128]{3,2,0,1:T(8,128)} %get-tuple-element.90) | copy-start | bytes 2359300
  109.2 14.9 %collective-permute-start = (f32[8,128,128]{2,1,0:T(8,128)S(1)}, f32[8,128,128]{2,1,0:T(8,128)S(1)}, u32[]{:S(2)}, u32[]{:S(2)}) collective-permute-start(f32[8,128,128]{2,1,0:T(8,128)S(1)} %convolution_add_fusion.12), channel_id=1, source_target_pairs={{0,4},{4,8},{8,12},{12,16},{16,20},{20,24},{24,28},{1,5},{5,9},{9,... | collective-permute-start | bytes 1572872 | tf_op jit(solution)/shard_map/while/body/eval_jaxpr/ppermute | solution.py:17
  124.8 15.1 %collective-permute-start = (f32[8,128,128]{2,1,0:T(8,128)S(1)}, f32[8,128,128]{2,1,0:T(8,128)S(1)}, u32[]{:S(2)}, u32[]{:S(2)}) collective-permute-start(f32[8,128,128]{2,1,0:T(8,128)S(1)} %convolution_add_fusion.12), channel_id=1, source_target_pairs={{0,4},{4,8},{8,12},{12,16},{16,20},{20,24},{24,28},{1,5},{5,9},{9,... | collective-permute-start | bytes 1572872 | tf_op jit(solution)/shard_map/while/body/eval_jaxpr/ppermute | solution.py:17
  140.6 14.2 %collective-permute-start = (f32[8,128,128]{2,1,0:T(8,128)S(1)}, f32[8,128,128]{2,1,0:T(8,128)S(1)}, u32[]{:S(2)}, u32[]{:S(2)}) collective-permute-start(f32[8,128,128]{2,1,0:T(8,128)S(1)} %convolution_add_fusion.12), channel_id=1, source_target_pairs={{0,4},{4,8},{8,12},{12,16},{16,20},{20,24},{24,28},{1,5},{5,9},{9,... | collective-permute-start | bytes 1572872 | tf_op jit(solution)/shard_map/while/body/eval_jaxpr/ppermute | solution.py:17
  155.5 14.2 %collective-permute-start = (f32[8,128,128]{2,1,0:T(8,128)S(1)}, f32[8,128,128]{2,1,0:T(8,128)S(1)}, u32[]{:S(2)}, u32[]{:S(2)}) collective-permute-start(f32[8,128,128]{2,1,0:T(8,128)S(1)} %convolution_add_fusion.12), channel_id=1, source_target_pairs={{0,4},{4,8},{8,12},{12,16},{16,20},{20,24},{24,28},{1,5},{5,9},{9,... | collective-permute-start | bytes 1572872 | tf_op jit(solution)/shard_map/while/body/eval_jaxpr/ppermute | solution.py:17
  170.3 13.4 %collective-permute-start = (f32[8,128,128]{2,1,0:T(8,128)S(1)}, f32[8,128,128]{2,1,0:T(8,128)S(1)}, u32[]{:S(2)}, u32[]{:S(2)}) collective-permute-start(f32[8,128,128]{2,1,0:T(8,128)S(1)} %convolution_add_fusion.12), channel_id=1, source_target_pairs={{0,4},{4,8},{8,12},{12,16},{16,20},{20,24},{24,28},{1,5},{5,9},{9,... | collective-permute-start | bytes 1572872 | tf_op jit(solution)/shard_map/while/body/eval_jaxpr/ppermute | solution.py:17
  184.4 12.6 %collective-permute-start = (f32[8,128,128]{2,1,0:T(8,128)S(1)}, f32[8,128,128]{2,1,0:T(8,128)S(1)}, u32[]{:S(2)}, u32[]{:S(2)}) collective-permute-start(f32[8,128,128]{2,1,0:T(8,128)S(1)} %convolution_add_fusion.12), channel_id=1, source_target_pairs={{0,4},{4,8},{8,12},{12,16},{16,20},{20,24},{24,28},{1,5},{5,9},{9,... | collective-permute-start | bytes 1572872 | tf_op jit(solution)/shard_map/while/body/eval_jaxpr/ppermute | solution.py:17
  197.7 12.0 %collective-permute-start = (f32[8,128,128]{2,1,0:T(8,128)S(1)}, f32[8,128,128]{2,1,0:T(8,128)S(1)}, u32[]{:S(2)}, u32[]{:S(2)}) collective-permute-start(f32[8,128,128]{2,1,0:T(8,128)S(1)} %convolution_add_fusion.12), channel_id=1, source_target_pairs={{0,4},{4,8},{8,12},{12,16},{16,20},{20,24},{24,28},{1,5},{5,9},{9,... | collective-permute-start | bytes 1572872 | tf_op jit(solution)/shard_map/while/body/eval_jaxpr/ppermute | solution.py:17
  213.3 1.9 copy-start.4
  213.8 62.4 %copy-start.9 = (f32[2,4,16]{2,1,0:T(4,128)S(1)}, f32[2,4,16]{2,1,0:T(4,128)}, u32[]{:S(2)}) copy-start(f32[2,4,16]{2,1,0:T(4,128)} %get-tuple-element.259) | copy-start | bytes 1540
  213.8 63.3 %copy-start.8 = (f32[2,4,16]{2,1,0:T(4,128)S(1)}, f32[2,4,16]{2,1,0:T(4,128)}, u32[]{:S(2)}) copy-start(f32[2,4,16]{2,1,0:T(4,128)} %get-tuple-element.260) | copy-start | bytes 1540
  213.8 83.9 %copy-start.7 = (bf16[2,4,128]{2,1,0:T(4,128)(2,1)S(1)}, bf16[2,4,128]{2,1,0:T(4,128)(2,1)}, u32[]{:S(2)}) copy-start(bf16[2,4,128]{2,1,0:T(4,128)(2,1)} %param.31) | copy-start | bytes 6148
  213.8 83.9 %copy-start.10 = (f32[2,4]{1,0:T(2,128)S(1)}, f32[2,4]{1,0:T(2,128)}, u32[]{:S(2)}) copy-start(f32[2,4]{1,0:T(2,128)} %param.33) | copy-start | bytes 100
  213.8 84.1 %copy-start.12 = (f32[128]{0:T(128)S(1)}, f32[128]{0:T(128)}, u32[]{:S(2)}) copy-start(f32[128]{0:T(128)} %param.28) | copy-start | bytes 1540
  (1 other events, 1.0 us)
Sparse Core Ops, SparseCore 0:
  9.5 31.2 all-gather.1
  211.1 64.9 reduce-scatter.1
where the time goes:
time: 306 us; the launch traced here: 305 us
  waiting for transfers between devices  151 us (49%)
  matrix products  71.6 us (23%)
  starting transfers between devices  33.5 us (11%)
  blocking collectives  19.8 us (6%)
  between operations  14.5 us (5%)
  other arithmetic  9.26 us (3%)
  local copies, waits for them, and re-layouts  5.57 us (2%)
    ppermute x7, waiting for transfers between devices, shifted(): lax.ppermute(value, axis, [(source, source + steps) for source in range(f...  63 us
    reduce_scatter x1, waiting for transfers between devices, shards(): lax.psum_scatter(own_term.astype(jnp.bfloat16), 'sp', scatter_dimension=2...  60 us
    dot_general x49, matrix products, matmul(): return jnp.einsum(form, left, right, precision=highest)  48.5 us
    ppermute x7, starting transfers between devices, shifted(): lax.ppermute(value, axis, [(source, source + steps) for source in range(f...  33.4 us
    all_gather x1, waiting for transfers between devices, shards(): lax.all_gather(tokens, 'tp', axis=2, tiled=True)  27.1 us
    dot_general x6, matrix products, project_rows(): jnp.dot(flat_rows, weight, preferred_element_type=jnp.float32)  23.1 us
    psum x1, blocking collectives, shards(): lax.psum((matmul('shde,shd->she', memory, query_part), matmul('shde,shd->...  19.8 us
  transfers between devices with their start and end apart: 9, of which 9 were waited for; matrix products, arithmetic and copies ran while one was open for 4% of the time, Pallas kernels for 0%

commit v1 on v0

v1 whole, which is shorter than its diff:
```python
import functools

import jax
import jax.numpy as jnp
from jax import lax
from jax.experimental import pallas as pl
from jax.experimental.pallas import tpu as pltpu
from jax.sharding import PartitionSpec as P

unit_floor = 1.0
norm_floor = 0.001
highest = lax.Precision.HIGHEST
MESH = pl.DeviceIdType.MESH
PAD = 8
f32 = jnp.float32
bf16 = jnp.bfloat16

NN = (((1,), (0,)), ((), ()))
NT = (((1,), (1,)), ((), ()))
TN = (((0,), (0,)), ((), ()))


def dot(left, right, dims=NN, precision=None):
    return lax.dot_general(left, right, dims, precision=precision, preferred_element_type=f32)


def gather_kernel(
    n, seqs, x_ref, wq_ref, wk_ref, wv_ref, wg_ref, bd_ref, out_ref, small_ref,
    xs, wbuf, acc, sacc, wsem, cross_sem, part_sem, fwd_sem, rx,
):
    me = lax.axis_index("tp")
    y, c = me // 2, lax.rem(me, 2)
    chips = n // 2
    rows, kd = x_ref.shape
    span = rows // seqs
    _, chunks, _, kc = xs.shape
    partner = y * 2 + (1 - c)
    weights = (wq_ref, wk_ref, wv_ref, wg_ref)

    barrier = pltpu.get_barrier_semaphore()
    pl.semaphore_signal(barrier, inc=1, device_id={"tp": partner}, device_id_type=MESH)
    for d in range(1, chips):
        to = lax.rem(y + d, chips) * 2 + c
        pl.semaphore_signal(barrier, inc=1, device_id={"tp": to}, device_id_type=MESH)

    order = [me, partner]
    for d in range(1, chips):
        source = lax.rem(y - d + chips, chips)
        order += [source * 2 + c, source * 2 + (1 - c)]

    def weight_copy(w, slot):
        start = pl.multiple_of(order[slot] * kd, kd)
        return pltpu.make_async_copy(
            weights[w].at[pl.ds(start, kd), :], wbuf.at[w, slot], wsem.at[w, slot]
        )

    for slot in range(n):
        for w in range(4):
            weight_copy(w, slot).start()
    pl.semaphore_wait(barrier, chips)

    def cols(ck):
        return pl.ds(ck * kc, kc)

    def cross_copy(d, ck):
        to = lax.rem(y + d, chips) * 2 + c
        return pltpu.make_async_remote_copy(
            src_ref=x_ref.at[:, cols(ck)], dst_ref=xs.at[me, ck],
            send_sem=cross_sem.at[d - 1, ck], recv_sem=rx.at[me, ck],
            device_id={"tp": to}, device_id_type=MESH,
        )

    def part_copy(ck):
        return pltpu.make_async_remote_copy(
            src_ref=x_ref.at[:, cols(ck)], dst_ref=xs.at[me, ck],
            send_sem=part_sem.at[ck], recv_sem=rx.at[me, ck],
            device_id={"tp": partner}, device_id_type=MESH,
        )

    def fwd_copy(d, ck):
        b = order[2 * d]
        return pltpu.make_async_remote_copy(
            src_ref=xs.at[b, ck], dst_ref=xs.at[b, ck],
            send_sem=fwd_sem.at[d - 1, ck], recv_sem=rx.at[b, ck],
            device_id={"tp": partner}, device_id_type=MESH,
        )

    def arrive(b, ck):
        pltpu.make_async_remote_copy(
            src_ref=xs.at[b, ck], dst_ref=xs.at[b, ck],
            send_sem=part_sem.at[ck], recv_sem=rx.at[b, ck],
            device_id={"tp": partner}, device_id_type=MESH,
        ).wait_recv()

    for ck in range(chunks):
        for d in range(1, chips):
            cross_copy(d, ck).start()
    for ck in range(chunks):
        part_copy(ck).start()

    def small(x, start, depth, first):
        piece = bd_ref[:, pl.ds(pl.multiple_of(start, depth), depth)]
        for s in range(seqs):
            term = dot(piece, x[s * span : (s + 1) * span], NT)
            sacc[s] = term if first else sacc[s] + term

    for w in range(4):
        weight_copy(w, 0).wait()
        acc[w] = dot(x_ref[...], wbuf[w, 0])
    small(x_ref[...], me * kd, kd, True)

    def use(slot, ck):
        b = order[slot]
        x = xs[b, ck]
        for w in range(4):
            if ck == 0:
                weight_copy(w, slot).wait()
            acc[w] += dot(x, wbuf[w, slot, pl.ds(ck * kc, kc), :])
        small(x, b * kd + ck * kc, kc, False)

    for ck in range(chunks):
        arrive(partner, ck)
        use(1, ck)
    for d in range(1, chips):
        for ck in range(chunks):
            arrive(order[2 * d], ck)
            fwd_copy(d, ck).start()
            use(2 * d, ck)
            arrive(order[2 * d + 1], ck)
            use(2 * d + 1, ck)
    for w in range(4):
        out_ref[w] = acc[w].astype(bf16)
    small_ref[...] = sacc[...]
    for ck in range(chunks):
        part_copy(ck).wait_send()
        for d in range(1, chips):
            cross_copy(d, ck).wait_send()
            fwd_copy(d, ck).wait_send()


def gather_project(n, seqs, tokens, weights, bd):
    rows, kd = tokens.shape
    width = weights[0].shape[1]
    kc = 256 if kd % 256 == 0 else kd
    chunks = kd // kc
    chips = n // 2
    span = rows // seqs
    return pl.pallas_call(
        functools.partial(gather_kernel, n, seqs),
        out_shape=(
            jax.ShapeDtypeStruct((4, rows, width), bf16),
            jax.ShapeDtypeStruct((seqs, 2 * PAD, span), f32),
        ),
        in_specs=[pl.BlockSpec(memory_space=pltpu.VMEM)]
        + [pl.BlockSpec(memory_space=pl.ANY)] * 4
        + [pl.BlockSpec(memory_space=pltpu.VMEM)],
        out_specs=(pl.BlockSpec(memory_space=pltpu.VMEM),) * 2,
        scratch_shapes=[
            pltpu.VMEM((n, chunks, rows, kc), bf16),
            pltpu.VMEM((4, n, kd, width), bf16),
            pltpu.VMEM((4, rows, width), f32),
            pltpu.VMEM((seqs, 2 * PAD, span), f32),
            pltpu.SemaphoreType.DMA((4, n)),
            pltpu.SemaphoreType.DMA((chips - 1, chunks)),
            pltpu.SemaphoreType.DMA((chunks,)),
            pltpu.SemaphoreType.DMA((chips - 1, chunks)),
            pltpu.SemaphoreType.DMA((n, chunks)),
        ],
        compiler_params=pltpu.CompilerParams(
            collective_id=0, has_side_effects=True, vmem_limit_bytes=60 * 1024 * 1024
        ),
    )(tokens, *weights, bd)


def unit_rows(values):
    return values * lax.rsqrt(jnp.sum(values * values, axis=-1, keepdims=True) + unit_floor)


def delta_kernel(
    n, seqs, heads, group, rows_ref, small_ref, par_ref, gain_ref, nq_ref, nk_ref, nv_ref,
    nb_ref, nd_ref, mixed_ref, cache_ref, first_ref,
    cum_row, cum_col, beta_col, local_out, reach, out_box, in_box, back_out, back_in, tail_out,
    tail_in, send1, recv1, send2, recv2, send3, recv3,
):
    me = lax.axis_index("sp")
    pairs = seqs * heads
    span = rows_ref.shape[1] // seqs
    extent = rows_ref.shape[2] // heads
    key_rows = extent // n

    barrier = pltpu.get_barrier_semaphore()
    for d in range(1, n):
        to = lax.rem(me + d, n)
        pl.semaphore_signal(barrier, inc=1, device_id={"sp": to}, device_id_type=MESH)

    row = lax.broadcasted_iota(jnp.int32, (span, span), 0)
    col = lax.broadcasted_iota(jnp.int32, (span, span), 1)
    upper = jnp.where(row <= col, 1.0, 0.0)
    bias, rate = par_ref[0:PAD], par_ref[PAD : 2 * PAD]
    for s in range(seqs):
        beta = jax.nn.sigmoid(small_ref[s, 0:PAD, :] + bias)
        pre = small_ref[s, PAD : 2 * PAD, :]
        soft = jnp.maximum(pre, 0.0) + jnp.log1p(jnp.exp(-jnp.abs(pre)))
        cum = dot(-jnp.exp(rate) * soft, upper, NN, highest)
        cum_row[s] = cum
        cum_col[s] = cum.T
        beta_col[s] = beta.T
    eye_lane = lax.broadcasted_iota(jnp.int32, (extent, extent), 0) == lax.broadcasted_iota(
        jnp.int32, (extent, extent), 1
    )
    pl.semaphore_wait(barrier, n - 1)

    def send_box(p):
        return pltpu.make_async_remote_copy(
            src_ref=out_box.at[p], dst_ref=in_box.at[me],
            send_sem=send1.at[p], recv_sem=recv1.at[me],
            device_id={"sp": p}, device_id_type=MESH,
        )

    def local_group(i, _):
        ps = [lax.rem(me + 1 + i * group + j, pairs) for j in range(group)]
        each = []
        for p in ps:
            s, h = p // heads, lax.rem(p, heads)
            at = pl.ds(pl.multiple_of(s * span, span), span)
            lanes = pl.ds(pl.multiple_of(h * extent, extent), extent)
            q = unit_rows(rows_ref[0, at, lanes].astype(f32))
            k = unit_rows(rows_ref[1, at, lanes].astype(f32))
            v = rows_ref[2, at, lanes].astype(f32)
            pick = lax.broadcasted_iota(jnp.int32, (span, PAD), 1) == h
            cumc = jnp.sum(jnp.where(pick, cum_col[s], 0.0), axis=1, keepdims=True)
            beta = jnp.sum(jnp.where(pick, beta_col[s], 0.0), axis=1, keepdims=True)
            cumr = cum_row[s, pl.ds(h, 1), :]
            causal = row >= col
            weights = jnp.where(causal, jnp.exp(jnp.where(causal, cumc - cumr, 0.0)), 0.0)
            kb = k * beta
            kh = k.astype(bf16)
            lower = jnp.where(row > col, dot(kb.astype(bf16), kh, NT) * weights, 0.0)
            score = (dot(q.astype(bf16), kh, NT) * weights).astype(bf16)
            grow = jnp.exp(cumc)
            right = jnp.concatenate([v * beta, kb * grow], axis=1).astype(bf16)
            last = cumc[span - 1 :, :]
            kdec = (k * jnp.exp(last - cumc)).astype(bf16)
            each.append([lower, score, right, kdec, q * grow, jnp.exp(last)])
        unit = jnp.where(row == col, 1.0, 0.0)
        pair_mask = ((row >> 1) == (col >> 1)) & (row > col)
        inv = [unit - jnp.where(pair_mask, e[0], 0.0) for e in each]
        level = 1
        while (1 << level) < span:
            mask = ((row >> (level + 1)) == (col >> (level + 1))) & ((row >> level) > (col >> level))
            inv_h = [m.astype(bf16) for m in inv]
            mid = [
                dot(jnp.where(mask, e[0], 0.0).astype(bf16), m).astype(bf16)
                for e, m in zip(each, inv_h)
            ]
            inv = [m - dot(mh, t) for m, mh, t in zip(inv, inv_h, mid)]
            level += 1
        uw = [dot(m.astype(bf16), e[2]).astype(bf16) for m, e in zip(inv, each)]
        out = [dot(e[1], u) for e, u in zip(each, uw)]
        fin = [dot(e[3], u, TN) for e, u in zip(each, uw)]
        for p, e, o, z in zip(ps, each, out, fin):
            local_out[p] = o[:, :extent]
            reach[p] = (e[4] - o[:, extent:]).astype(bf16)
            step = (jnp.where(eye_lane, e[5] - 1.0, 0.0) - z[:, extent:]).astype(bf16)
            state = z[:, :extent].astype(bf16)

            @pl.when(p == me)
            def _():
                in_box[me, 0] = step
                in_box[me, 1] = state

            @pl.when(p != me)
            def _():
                out_box[p, 0] = step
                out_box[p, 1] = state
                send_box(p).start()

        return 0

    lax.fori_loop(0, pairs // group, local_group, 0)

    def back_copy(j):
        return pltpu.make_async_remote_copy(
            src_ref=back_out.at[j], dst_ref=back_in.at[me],
            send_sem=send2.at[j], recv_sem=recv2.at[me],
            device_id={"sp": j}, device_id_type=MESH,
        )

    def tail_copy(j):
        return pltpu.make_async_remote_copy(
            src_ref=tail_out.at[j], dst_ref=tail_in.at[me],
            send_sem=send3.at[j], recv_sem=recv3.at[me],
            device_id={"sp": j}, device_id_type=MESH,
        )

    @pl.when(me < pairs)
    def _():
        def chain(j, state):
            half = state.astype(bf16)

            @pl.when(j == me)
            def _():
                back_in[me] = half

            @pl.when(j != me)
            def _():
                back_out[j] = half
                back_copy(j).start()
                pltpu.make_async_remote_copy(
                    src_ref=out_box.at[0], dst_ref=in_box.at[j],
                    send_sem=send1.at[0], recv_sem=recv1.at[j],
                    device_id={"sp": j}, device_id_type=MESH,
                ).wait_recv()

            return state + dot(in_box[j, 0], half) + in_box[j, 1].astype(f32)

        final = lax.fori_loop(0, n, chain, jnp.zeros((extent, extent), f32))
        memory = final.astype(bf16).astype(f32)
        shape3 = nq_ref.shape
        mine = (
            lax.broadcasted_iota(jnp.int32, shape3, 0) * heads
            + lax.broadcasted_iota(jnp.int32, shape3, 1)
        ) == me

        def own(ref):
            kept = jnp.where(mine, ref[...].astype(f32), 0.0)
            return jnp.sum(jnp.sum(kept, axis=0), axis=0, keepdims=True)

        qn, kn = unit_rows(own(nq_ref)), unit_rows(own(nk_ref))
        both = jnp.concatenate([jnp.broadcast_to(qn, (PAD, extent)), jnp.broadcast_to(kn, (PAD, extent))], axis=0)
        reads = dot(both, memory, NN, highest)
        recall, retrieve = reads[0:1], reads[PAD : PAD + 1]
        s, h = me // heads, lax.rem(me, heads)
        beta_new, decay_new = nb_ref[s, h], nd_ref[s, h]
        fresh = own(nv_ref) - decay_new * retrieve
        meet = jnp.sum(kn * qn, axis=-1, keepdims=True)
        read = decay_new * recall + (beta_new * meet) * fresh
        norm = lax.rsqrt(jnp.mean(read * read, axis=-1, keepdims=True) + norm_floor)
        answer = jnp.broadcast_to(read * norm * gain_ref[...], (PAD, extent))
        for j in range(n):
            tail_out[j, 0:key_rows, :] = memory[j * key_rows : (j + 1) * key_rows]
            tail_out[j, tail_out.shape[1] - PAD :, :] = answer

        def push(j, _):
            @pl.when(j == me)
            def _():
                tail_in[me] = tail_out[me]

            @pl.when(j != me)
            def _():
                tail_copy(j).start()

            return 0

        lax.fori_loop(0, n, push, 0)

    gain = gain_ref[...]

    def finish(i, _):
        p = lax.rem(me + i, pairs)
        s, h = p // heads, lax.rem(p, heads)
        at = pl.ds(pl.multiple_of(s * span, span), span)
        lanes = pl.ds(pl.multiple_of(h * extent, extent), extent)

        @pl.when(p != me)
        def _():
            pltpu.make_async_remote_copy(
                src_ref=back_out.at[0], dst_ref=back_in.at[p],
                send_sem=send2.at[0], recv_sem=recv2.at[p],
                device_id={"sp": p}, device_id_type=MESH,
            ).wait_recv()

        o = local_out[p] + dot(reach[p], back_in[p])
        norm = lax.rsqrt(jnp.mean(o * o, axis=-1, keepdims=True) + norm_floor)
        gate = rows_ref[3, at, lanes].astype(f32)
        mixed_ref[at, lanes] = (o * norm * gain * (gate * jax.nn.sigmoid(gate))).astype(bf16)
        return 0

    lax.fori_loop(0, pairs, finish, 0)

    for p in range(pairs):

        @pl.when(p != me)
        def _():
            pltpu.make_async_remote_copy(
                src_ref=tail_out.at[0], dst_ref=tail_in.at[p],
                send_sem=send3.at[0], recv_sem=recv3.at[p],
                device_id={"sp": p}, device_id_type=MESH,
            ).wait_recv()

        cache_ref[p] = tail_in[p, 0:key_rows, :].astype(bf16)
        last = tail_in.shape[1]
        first_ref[p : p + 1, :] = tail_in[p, last - PAD : last - PAD + 1, :]

    for p in range(pairs):

        @pl.when(p != me)
        def _():
            send_box(p).wait_send()

    @pl.when(me < pairs)
    def _():
        for j in range(n):

            @pl.when(j != me)
            def _():
                back_copy(j).wait_send()
                tail_copy(j).wait_send()


def delta(n, seqs, heads, rows4, small, par, gain, nq, nk, nv, nb, nd):
    _, rows, width = rows4.shape
    span, extent = rows // seqs, width // heads
    pairs = seqs * heads
    key_rows = extent // n
    tail = -(-key_rows // PAD) * PAD + PAD
    vmem = pl.BlockSpec(memory_space=pltpu.VMEM)
    smem = pl.BlockSpec(memory_space=pltpu.SMEM)
    return pl.pallas_call(
        functools.partial(delta_kernel, n, seqs, heads, 2),
        out_shape=(
            jax.ShapeDtypeStruct((rows, width), bf16),
            jax.ShapeDtypeStruct((pairs, key_rows, extent), bf16),
            jax.ShapeDtypeStruct((pairs, extent), f32),
        ),
        in_specs=[vmem] * 7 + [smem] * 2,
        out_specs=(vmem,) * 3,
        scratch_shapes=[
            pltpu.VMEM((seqs, PAD, span), f32),
            pltpu.VMEM((seqs, span, PAD), f32),
            pltpu.VMEM((seqs, span, PAD), f32),
            pltpu.VMEM((pairs, span, extent), f32),
            pltpu.VMEM((pairs, span, extent), bf16),
            pltpu.VMEM((pairs, 2, extent, extent), bf16),
            pltpu.VMEM((n, 2, extent, extent), bf16),
            pltpu.VMEM((n, extent, extent), bf16),
            pltpu.VMEM((pairs, extent, extent), bf16),
            pltpu.VMEM((n, tail, extent), f32),
            pltpu.VMEM((pairs, tail, extent), f32),
            pltpu.SemaphoreType.DMA((pairs,)),
            pltpu.SemaphoreType.DMA((n,)),
            pltpu.SemaphoreType.DMA((n,)),
            pltpu.SemaphoreType.DMA((pairs,)),
            pltpu.SemaphoreType.DMA((n,)),
            pltpu.SemaphoreType.DMA((pairs,)),
        ],
        compiler_params=pltpu.CompilerParams(
            collective_id=1, has_side_effects=True, vmem_limit_bytes=48 * 1024 * 1024
        ),
    )(rows4, small, par, gain, nq, nk, nv, nb, nd)


def shards(
    tokens, query_weight, key_weight, value_weight, gate_weight, beta_weight, decay_weight,
    beta_bias, rate_log, out_gain, new_query, new_key, new_value, new_beta, new_decay,
):
    seqs, span, kd = tokens.shape
    heads = rate_log.shape[0]
    extent = out_gain.shape[0]
    tp, sp = lax.axis_size("tp"), lax.axis_size("sp")
    fill = ((0, PAD - heads), (0, 0))
    bd = jnp.concatenate([jnp.pad(beta_weight.T, fill), jnp.pad(decay_weight.T, fill)], axis=0)
    par = jnp.concatenate(
        [jnp.pad(beta_bias[:, None], fill), jnp.pad(rate_log[:, None], fill)], axis=0
    )
    weights = (query_weight, key_weight, value_weight, gate_weight)
    rows4, small = gather_project(tp, seqs, tokens.reshape(seqs * span, kd), weights, bd)
    mixed, cache, first = delta(
        sp, seqs, heads, rows4, small, par, out_gain[None], new_query, new_key, new_value,
        new_beta, new_decay,
    )
    return (
        mixed.reshape(seqs, span, heads * extent),
        cache.reshape(seqs, heads, extent // sp, extent),
        first.reshape(seqs, heads * extent),
    )


def solution(mesh):
    placed = (
        P(None, "sp", "tp"),
        P(None, "tp"),
        P(None, "tp"),
        P(None, "tp"),
        P(None, "tp"),
        P(None, "tp"),
        P(None, "tp"),
        P("tp"),
        P("tp"),
        P(),
        P(None, "tp", None),
        P(None, "tp", None),
        P(None, "tp", None),
        P(None, "tp"),
        P(None, "tp"),
    )
    return jax.shard_map(
        shards,
        mesh=mesh,
        in_specs=placed,
        out_specs=(P(None, "sp", "tp"), P(None, "tp", "sp", None), P(None, "tp")),
        check_vma=False,
    )
```

time: 306 us -> 64.6 us (0.21)
  waiting for transfers between devices: 151 us -> 0 us
  matrix products: 71.6 us -> 0 us
  Pallas kernels: 0 us -> 56.8 us
  starting transfers between devices: 33.5 us -> 0 us
  blocking collectives: 19.8 us -> 0 us
  between operations: 14.5 us -> 0.73 us
  other arithmetic: 9.26 us -> 2.2 us
    dot_general x55 -> x0, matrix products: 71.6 us -> none  [the longest x49 48.5 us: matmul(): return jnp.einsum(form, left, right, precision=highest)]
    ppermute x7 -> x0, waiting for transfers between devices: 63 us -> none  [shifted(): lax.ppermute(value, axis, [(source, source + steps) for source in range(f...]
    reduce_scatter x1 -> x0, waiting for transfers between devices: 60 us -> none  [shards(): lax.psum_scatter(own_term.astype(jnp.bfloat16), 'sp', scatter_dimension=2...]
    pallas_call x0 -> x2, Pallas kernels: none -> 56.8 us  [the longest x1 30.9 us: delta(): pl.pallas_call(functools.partial(delta_kernel, n, seqs, heads, 2), out_sh...]
    ppermute x7 -> x0, starting transfers between devices: 33.4 us -> none  [shifted(): lax.ppermute(value, axis, [(source, source + steps) for source in range(f...]
    all_gather x1 -> x0, waiting for transfers between devices: 27.1 us -> none  [shards(): lax.all_gather(tokens, 'tp', axis=2, tiled=True)]
    psum x1 -> x0, blocking collectives: 19.8 us -> none  [shards(): lax.psum((matmul('shde,shd->she', memory, query_part), matmul('shde,shd->...]
    reduce_sum x7 -> x0, other arithmetic: 3.8 us -> none  [the longest x4 2.49 us: unit_rows(): jnp.sum(values * values, axis=-1, keepdims=True) + unit_floor]
  transfers between devices with their start and end apart: 9 -> 0, of which waited for: 9 -> 0; matrix products, arithmetic and copies ran while one was open for 4% -> 0% of each run, Pallas kernels for 0% -> 0%
where the time goes in v1:
time: 64.6 us; the launch traced here: 63.9 us
  Pallas kernels  56.8 us (88%)
  local copies, waits for them, and re-layouts  4.23 us (7%)
  other arithmetic  2.2 us (3%)
  between operations  0.73 us (1%)
    pallas_call x1, Pallas kernels, delta(): pl.pallas_call(functools.partial(delta_kernel, n, seqs, heads, 2), out_sh...  30.9 us
    pallas_call x1, Pallas kernels, gather_project(): pl.pallas_call(functools.partial(gather_kernel, n, seqs), out_shape=(jax....  25.8 us
    unnamed x18, local copies, waits for them, and re-layouts  3.55 us
    concatenate x1, other arithmetic, shards(): jnp.concatenate([jnp.pad(beta_weight.T, fill), jnp.pad(decay_weight.T, fi...  1.45 us

profile of v1, /device:TPU:0, one launch (start us, length us, event | category | flops | bytes accessed | tf_op | source)
XLA Modules:
  0.0 63.9 jit_solution(8734607252256816748)
XLA Ops:
  0.6 0.7 %fusion.3 = f32[16,1]{0,1:T(1,128)S(1)} fusion(f32[4,1]{0,1:T(1,128)} %bitcast.14, f32[4,1]{0,1:T(1,128)} %bitcast.15), kind=kLoop, calls=%fused_computation.7 | loop fusion | flops 80 | bytes 96 | tf_op jit(solution)/shard_map/concatenate | solution.py:463
  1.4 0.1 copy.20.par_ref
  1.5 1.5 %fusion.2.bd_ref = bf16[16,4096]{1,0:T(8,128)(2,1)} fusion(bf16[4,4096]{1,0:T(4,128)(2,1)} %bitcast.12, bf16[4,4096]{1,0:T(4,128)(2,1)} %bitcast.13), kind=kLoop, calls=%fused_computation.4 | loop fusion | flops 524288 | bytes 196608 | tf_op jit(solution)/shard_map/concatenate | solution.py:462
  2.9 0.0 copy-start.2
  2.9 0.0 copy-start.3
  2.9 0.0 copy-start.4
  2.9 0.0 copy-start.5
  2.9 0.0 copy-start.6
  2.9 0.0 copy-start.7
  3.0 25.8 %shard_map.166 = (bf16[4,384,512]{2,1,0:T(8,128)(2,1)}, f32[2,16,192]{2,1,0:T(8,128)}) custom-call(bf16[384,1024]{1,0:T(8,128)(2,1)} %bitcast.11, bf16[4096,512]{1,0:T(8,128)(2,1)} %wq_ref.1, bf16[4096,512]{1,0:T(8,128)(2,1)} %wk_ref.1, bf16[4096,512]{1,0:T(8,128)(2,1)} %wv_ref.1, bf16[4096,512]{1,0:T(8,128)(2,1)} %wg_ref.1, bf16[16,4096]{1,0:T(8,128)(2,1)} %fusion.2.bd_ref), custom_call_target="tpu_custom_call" | custom-call | tf_op jit(solution)/shard_map/pallas_call | solution.py:148
  28.8 0.0 copy-done.2
  28.8 0.0 copy-done.3
  28.8 0.0 copy-done.4
  28.8 0.0 copy-done.5
  28.8 0.0 copy-done.6
  28.8 0.0 copy-done.7
  28.8 0.0 copy-start
  28.9 1.4 %copy-done = bf16[4,384,512]{2,1,0:T(8,128)(2,1)S(1)} copy-done((bf16[4,384,512]{2,1,0:T(8,128)(2,1)S(1)}, bf16[4,384,512]{2,1,0:T(8,128)(2,1)}, u32[]{:S(2)}) %copy-start) | copy-done | bytes 1572888
  30.3 0.0 copy-start.1
  30.3 0.8 %copy-done.1 = f32[2,16,192]{2,1,0:T(8,128)S(1)} copy-done((f32[2,16,192]{2,1,0:T(8,128)S(1)}, f32[2,16,192]{2,1,0:T(8,128)}, u32[]{:S(2)}) %copy-start.1) | copy-done | bytes 24600
  31.0 30.9 %shard_map.167 = (bf16[384,512]{1,0:T(8,128)(2,1)S(1)}, bf16[8,16,128]{2,1,0:T(8,128)(2,1)S(1)}, f32[8,128]{1,0:T(8,128)S(1)}) custom-call(bf16[4,384,512]{2,1,0:T(8,128)(2,1)S(1)} %copy-done, f32[2,16,192]{2,1,0:T(8,128)S(1)} %copy-done.1, f32[16,1]{1,0:T(8,128)S(1)} %copy.20.par_ref, f32[1,128]{1,0:T(1,128)S(1)} %bitcast.10, ...), custom_call_target="tpu_custom_call" | custom-call | tf_op jit(solution)/shard_map/pallas_call | solution.py:419
  62.0 0.6 reshape.21
  62.6 0.7 %copy.23 = bf16[2,192,512]{2,1,0:T(8,128)(2,1)} copy(bf16[2,192,512]{2,1,0:T(8,128)(2,1)S(1)} %bitcast.8) | data formatting | bytes 786432
  63.3 0.6 copy.24
Async XLA Ops:
  2.9 25.9 %copy-start.2 = (bf16[2,4,128]{2,1,0:T(4,128)(2,1)S(1)}, bf16[2,4,128]{2,1,0:T(4,128)(2,1)}, u32[]{:S(2)}) copy-start(bf16[2,4,128]{2,1,0:T(4,128)(2,1)} %nq_ref.1) | copy-start | bytes 6148
  2.9 25.9 %copy-start.3 = (bf16[2,4,128]{2,1,0:T(4,128)(2,1)S(1)}, bf16[2,4,128]{2,1,0:T(4,128)(2,1)}, u32[]{:S(2)}) copy-start(bf16[2,4,128]{2,1,0:T(4,128)(2,1)} %nk_ref.1) | copy-start | bytes 6148
  2.9 25.9 %copy-start.4 = (bf16[2,4,128]{2,1,0:T(4,128)(2,1)S(1)}, bf16[2,4,128]{2,1,0:T(4,128)(2,1)}, u32[]{:S(2)}) copy-start(bf16[2,4,128]{2,1,0:T(4,128)(2,1)} %nv_ref.1) | copy-start | bytes 6148
  2.9 25.9 %copy-start.5 = (f32[2,4]{1,0:T(2,128)S(1)}, f32[2,4]{1,0:T(2,128)}, u32[]{:S(2)}) copy-start(f32[2,4]{1,0:T(2,128)} %nb_ref.1) | copy-start | bytes 100
  2.9 25.9 %copy-start.6 = (f32[2,4]{1,0:T(2,128)S(1)}, f32[2,4]{1,0:T(2,128)}, u32[]{:S(2)}) copy-start(f32[2,4]{1,0:T(2,128)} %nd_ref.1) | copy-start | bytes 100
  2.9 25.9 %copy-start.7 = (f32[128]{0:T(128)S(1)}, f32[128]{0:T(128)}, u32[]{:S(2)}) copy-start(f32[128]{0:T(128)} %param.24) | copy-start | bytes 1540
  28.8 1.4 %copy-start = (bf16[4,384,512]{2,1,0:T(8,128)(2,1)S(1)}, bf16[4,384,512]{2,1,0:T(8,128)(2,1)}, u32[]{:S(2)}) copy-start(bf16[4,384,512]{2,1,0:T(8,128)(2,1)} %get-tuple-element.8.rows_ref) | copy-start | bytes 4718596
  30.3 0.8 %copy-start.1 = (f32[2,16,192]{2,1,0:T(8,128)S(1)}, f32[2,16,192]{2,1,0:T(8,128)}, u32[]{:S(2)}) copy-start(f32[2,16,192]{2,1,0:T(8,128)} %get-tuple-element.9.small_ref) | copy-start | bytes 73732

commit v2 on v1

--- a/solution.py
+++ b/solution.py
@@ -24,191 +24,165 @@
     return lax.dot_general(left, right, dims, precision=precision, preferred_element_type=f32)
 
 
-def gather_kernel(
-    n, seqs, x_ref, wq_ref, wk_ref, wv_ref, wg_ref, bd_ref, out_ref, small_ref,
-    xs, wbuf, acc, sacc, wsem, cross_sem, part_sem, fwd_sem, rx,
+def unit_rows(values):
+    return values * lax.rsqrt(jnp.sum(values * values, axis=-1, keepdims=True) + unit_floor)
+
+
+def kernel(
+    n, tp, group,
+    x_hbm, wq_ref, wk_ref, wv_ref, wg_ref, bw_ref, dw_ref, bias_ref, rate_ref, gain_ref, nq_ref,
+    nk_ref, nv_ref, nb_ref, nd_ref, mixed_ref, cache_ref, first_ref,
+    x_ref, xs, wbuf, acc, sacc, bd, rows_ref,
+    cum_row, cum_col, beta_col, local_out, reach, out_box, in_box, back_out, back_in, tail_out,
+    tail_in, xsem, wsem, cross_sem, part_sem, fwd_sem, rx, send1, recv1, send2, recv2, send3, recv3,
 ):
-    me = lax.axis_index("tp")
-    y, c = me // 2, lax.rem(me, 2)
-    chips = n // 2
-    rows, kd = x_ref.shape
-    span = rows // seqs
-    _, chunks, _, kc = xs.shape
+    me = lax.axis_index("sp")
+    seqs, span, kd = x_hbm.shape
+    heads, = bias_ref.shape
+    pairs = seqs * heads
+    extent = rows_ref.shape[2] // heads
+    key_rows = extent // n
+    rank = lax.axis_index("tp")
+    y, c = rank // 2, lax.rem(rank, 2)
+    chips = tp // 2
+    _, _, chunks, _, kc = xs.shape
     partner = y * 2 + (1 - c)
-    weights = (wq_ref, wk_ref, wv_ref, wg_ref)
+    big = (wq_ref, wk_ref, wv_ref, wg_ref)
 
     barrier = pltpu.get_barrier_semaphore()
     pl.semaphore_signal(barrier, inc=1, device_id={"tp": partner}, device_id_type=MESH)
     for d in range(1, chips):
         to = lax.rem(y + d, chips) * 2 + c
         pl.semaphore_signal(barrier, inc=1, device_id={"tp": to}, device_id_type=MESH)
-
-    order = [me, partner]
+    for d in range(1, n):
+        to = lax.rem(me + d, n)
+        pl.semaphore_signal(barrier, inc=1, device_id={"sp": to}, device_id_type=MESH)
+
+    order = [rank, partner]
     for d in range(1, chips):
         source = lax.rem(y - d + chips, chips)
         order += [source * 2 + c, source * 2 + (1 - c)]
 
+    def token_copy(s):
+        return pltpu.make_async_copy(x_hbm.at[s], x_ref.at[s], xsem.at[s])
+
     def weight_copy(w, slot):
         start = pl.multiple_of(order[slot] * kd, kd)
         return pltpu.make_async_copy(
-            weights[w].at[pl.ds(start, kd), :], wbuf.at[w, slot], wsem.at[w, slot]
-        )
-
-    for slot in range(n):
+            big[w].at[pl.ds(start, kd), :], wbuf.at[w, slot], wsem.at[w, slot]
+        )
+
+    for s in range(seqs):
+        token_copy(s).start()
+    for slot in range(tp):
         for w in range(4):
             weight_copy(w, slot).start()
-    pl.semaphore_wait(barrier, chips)
+    bd[...] = jnp.zeros_like(bd)
+    bd[0:heads] = bw_ref[...]
+    bd[PAD : PAD + heads] = dw_ref[...]
 
     def cols(ck):
         return pl.ds(ck * kc, kc)
 
-    def cross_copy(d, ck):
+    def cross_copy(d, s, ck):
         to = lax.rem(y + d, chips) * 2 + c
         return pltpu.make_async_remote_copy(
-            src_ref=x_ref.at[:, cols(ck)], dst_ref=xs.at[me, ck],
-            send_sem=cross_sem.at[d - 1, ck], recv_sem=rx.at[me, ck],
+            src_ref=x_ref.at[s, :, cols(ck)], dst_ref=xs.at[rank, s, ck],
+            send_sem=cross_sem.at[d - 1, s, ck], recv_sem=rx.at[rank, s, ck],
             device_id={"tp": to}, device_id_type=MESH,
         )
 
-    def part_copy(ck):
-        return pltpu.make_async_remote_copy(
-            src_ref=x_ref.at[:, cols(ck)], dst_ref=xs.at[me, ck],
-            send_sem=part_sem.at[ck], recv_sem=rx.at[me, ck],
+    def part_copy(s, ck):
+        return pltpu.make_async_remote_copy(
+            src_ref=x_ref.at[s, :, cols(ck)], dst_ref=xs.at[rank, s, ck],
+            send_sem=part_sem.at[s, ck], recv_sem=rx.at[rank, s, ck],
             device_id={"tp": partner}, device_id_type=MESH,
         )
 
-    def fwd_copy(d, ck):
+    def fwd_copy(d, s, ck):
         b = order[2 * d]
         return pltpu.make_async_remote_copy(
-            src_ref=xs.at[b, ck], dst_ref=xs.at[b, ck],
-            send_sem=fwd_sem.at[d - 1, ck], recv_sem=rx.at[b, ck],
+            src_ref=xs.at[b, s, ck], dst_ref=xs.at[b, s, ck],
+            send_sem=fwd_sem.at[d - 1, s, ck], recv_sem=rx.at[b, s, ck],
             device_id={"tp": partner}, device_id_type=MESH,
         )
 
-    def arrive(b, ck):
+    def arrive(b, s, ck):
         pltpu.make_async_remote_copy(
-            src_ref=xs.at[b, ck], dst_ref=xs.at[b, ck],
-            send_sem=part_sem.at[ck], recv_sem=rx.at[b, ck],
+            src_ref=xs.at[b, s, ck], dst_ref=xs.at[b, s, ck],
+            send_sem=part_sem.at[s, ck], recv_sem=rx.at[b, s, ck],
             device_id={"tp": partner}, device_id_type=MESH,
         ).wait_recv()
 
-    for ck in range(chunks):
-        for d in range(1, chips):
-            cross_copy(d, ck).start()
-    for ck in range(chunks):
-        part_copy(ck).start()
-
-    def small(x, start, depth, first):
-        piece = bd_ref[:, pl.ds(pl.multiple_of(start, depth), depth)]
-        for s in range(seqs):
-            term = dot(piece, x[s * span : (s + 1) * span], NT)
-            sacc[s] = term if first else sacc[s] + term
+    token_copy(0).wait()
+    pl.semaphore_wait(barrier, chips + n - 1)
+    for s in range(seqs):
+        if s:
+            token_copy(s).wait()
+        for ck in range(chunks):
+            for d in range(1, chips):
+                cross_copy(d, s, ck).start()
+    for s in range(seqs):
+        for ck in range(chunks):
+            part_copy(s, ck).start()
+
+    row = lax.broadcasted_iota(jnp.int32, (span, span), 0)
+    col = lax.broadcasted_iota(jnp.int32, (span, span), 1)
+    eye_lane = lax.broadcasted_iota(jnp.int32, (extent, extent), 0) == lax.broadcasted_iota(
+        jnp.int32, (extent, extent), 1
+    )
+    slot_of = lax.broadcasted_iota(jnp.int32, (PAD, 1), 0)
+    bias = jnp.zeros((PAD, 1), f32)
+    rate = jnp.zeros((PAD, 1), f32)
+    for h in range(heads):
+        bias = jnp.where(slot_of == h, bias_ref[h], bias)
+        rate = jnp.where(slot_of == h, rate_ref[h], rate)
+
+    def small(x, s, start, depth, first):
+        term = dot(bd[:, pl.ds(pl.multiple_of(start, depth), depth)], x, NT)
+        sacc[s] = term if first else sacc[s] + term
+
+    def at_rows(s):
+        return pl.ds(s * span, span)
 
     for w in range(4):
         weight_copy(w, 0).wait()
-        acc[w] = dot(x_ref[...], wbuf[w, 0])
-    small(x_ref[...], me * kd, kd, True)
-
-    def use(slot, ck):
+        for s in range(seqs):
+            acc[w, at_rows(s)] = dot(x_ref[s], wbuf[w, 0])
+    for s in range(seqs):
+        small(x_ref[s], s, rank * kd, kd, True)
+
+    def use(slot, s, ck):
         b = order[slot]
-        x = xs[b, ck]
+        x = xs[b, s, ck]
         for w in range(4):
-            if ck == 0:
+            if ck == 0 and s == 0:
                 weight_copy(w, slot).wait()
-            acc[w] += dot(x, wbuf[w, slot, pl.ds(ck * kc, kc), :])
-        small(x, b * kd + ck * kc, kc, False)
-
-    for ck in range(chunks):
-        arrive(partner, ck)
-        use(1, ck)
-    for d in range(1, chips):
+            acc[w, at_rows(s)] += dot(x, wbuf[w, slot, pl.ds(ck * kc, kc), :])
+        small(x, s, b * kd + ck * kc, kc, False)
+
+    for s in range(seqs):
         for ck in range(chunks):
-            arrive(order[2 * d], ck)
-            fwd_copy(d, ck).start()
-            use(2 * d, ck)
-            arrive(order[2 * d + 1], ck)
-            use(2 * d + 1, ck)
-    for w in range(4):
-        out_ref[w] = acc[w].astype(bf16)
-    small_ref[...] = sacc[...]
-    for ck in range(chunks):
-        part_copy(ck).wait_send()
+            arrive(partner, s, ck)
+            use(1, s, ck)
+
+    def project(s):
         for d in range(1, chips):
-            cross_copy(d, ck).wait_send()
-            fwd_copy(d, ck).wait_send()
-
-
-def gather_project(n, seqs, tokens, weights, bd):
-    rows, kd = tokens.shape
-    width = weights[0].shape[1]
-    kc = 256 if kd % 256 == 0 else kd
-    chunks = kd // kc
-    chips = n // 2
-    span = rows // seqs
-    return pl.pallas_call(
-        functools.partial(gather_kernel, n, seqs),
-        out_shape=(
-            jax.ShapeDtypeStruct((4, rows, width), bf16),
-            jax.ShapeDtypeStruct((seqs, 2 * PAD, span), f32),
-        ),
-        in_specs=[pl.BlockSpec(memory_space=pltpu.VMEM)]
-        + [pl.BlockSpec(memory_space=pl.ANY)] * 4
-        + [pl.BlockSpec(memory_space=pltpu.VMEM)],
-        out_specs=(pl.BlockSpec(memory_space=pltpu.VMEM),) * 2,
-        scratch_shapes=[
-            pltpu.VMEM((n, chunks, rows, kc), bf16),
-            pltpu.VMEM((4, n, kd, width), bf16),
-            pltpu.VMEM((4, rows, width), f32),
-            pltpu.VMEM((seqs, 2 * PAD, span), f32),
-            pltpu.SemaphoreType.DMA((4, n)),
-            pltpu.SemaphoreType.DMA((chips - 1, chunks)),
-            pltpu.SemaphoreType.DMA((chunks,)),
-            pltpu.SemaphoreType.DMA((chips - 1, chunks)),
-            pltpu.SemaphoreType.DMA((n, chunks)),
-        ],
-        compiler_params=pltpu.CompilerParams(
-            collective_id=0, has_side_effects=True, vmem_limit_bytes=60 * 1024 * 1024
-        ),
-    )(tokens, *weights, bd)
-
-
-def unit_rows(values):
-    return values * lax.rsqrt(jnp.sum(values * values, axis=-1, keepdims=True) + unit_floor)
-
-
-def delta_kernel(
-    n, seqs, heads, group, rows_ref, small_ref, par_ref, gain_ref, nq_ref, nk_ref, nv_ref,
-    nb_ref, nd_ref, mixed_ref, cache_ref, first_ref,
-    cum_row, cum_col, beta_col, local_out, reach, out_box, in_box, back_out, back_in, tail_out,
-    tail_in, send1, recv1, send2, recv2, send3, recv3,
-):
-    me = lax.axis_index("sp")
-    pairs = seqs * heads
-    span = rows_ref.shape[1] // seqs
-    extent = rows_ref.shape[2] // heads
-    key_rows = extent // n
-
-    barrier = pltpu.get_barrier_semaphore()
-    for d in range(1, n):
-        to = lax.rem(me + d, n)
-        pl.semaphore_signal(barrier, inc=1, device_id={"sp": to}, device_id_type=MESH)
-
-    row = lax.broadcasted_iota(jnp.int32, (span, span), 0)
-    col = lax.broadcasted_iota(jnp.int32, (span, span), 1)
-    upper = jnp.where(row <= col, 1.0, 0.0)
-    bias, rate = par_ref[0:PAD], par_ref[PAD : 2 * PAD]
-    for s in range(seqs):
-        beta = jax.nn.sigmoid(small_ref[s, 0:PAD, :] + bias)
-        pre = small_ref[s, PAD : 2 * PAD, :]
+            for ck in range(chunks):
+                arrive(order[2 * d], s, ck)
+                fwd_copy(d, s, ck).start()
+                use(2 * d, s, ck)
+                arrive(order[2 * d + 1], s, ck)
+                use(2 * d + 1, s, ck)
+        for w in range(4):
+            rows_ref[w, at_rows(s)] = acc[w, at_rows(s)].astype(bf16)
+        beta = jax.nn.sigmoid(sacc[s, 0:PAD, :] + bias)
+        pre = sacc[s, PAD : 2 * PAD, :]
         soft = jnp.maximum(pre, 0.0) + jnp.log1p(jnp.exp(-jnp.abs(pre)))
-        cum = dot(-jnp.exp(rate) * soft, upper, NN, highest)
+        cum = dot(-jnp.exp(rate) * soft, jnp.where(row <= col, 1.0, 0.0), NN, highest)
         cum_row[s] = cum
         cum_col[s] = cum.T
         beta_col[s] = beta.T
-    eye_lane = lax.broadcasted_iota(jnp.int32, (extent, extent), 0) == lax.broadcasted_iota(
-        jnp.int32, (extent, extent), 1
-    )
-    pl.semaphore_wait(barrier, n - 1)
 
     def send_box(p):
         return pltpu.make_async_remote_copy(
@@ -217,12 +191,12 @@
             device_id={"sp": p}, device_id_type=MESH,
         )
 
-    def local_group(i, _):
-        ps = [lax.rem(me + 1 + i * group + j, pairs) for j in range(group)]
+    def local_group(s0, i, _):
+        ps = [s0 * heads + lax.rem(me + 1 + i * group + j, heads) for j in range(group)]
         each = []
         for p in ps:
-            s, h = p // heads, lax.rem(p, heads)
-            at = pl.ds(pl.multiple_of(s * span, span), span)
+            s, h = s0, lax.rem(p, heads)
+            at = at_rows(s)
             lanes = pl.ds(pl.multiple_of(h * extent, extent), extent)
             q = unit_rows(rows_ref[0, at, lanes].astype(f32))
             k = unit_rows(rows_ref[1, at, lanes].astype(f32))
@@ -277,7 +251,9 @@
 
         return 0
 
-    lax.fori_loop(0, pairs // group, local_group, 0)
+    for s in range(seqs):
+        project(s)
+        lax.fori_loop(0, heads // group, functools.partial(local_group, s), 0)
 
     def back_copy(j):
         return pltpu.make_async_remote_copy(
@@ -406,26 +382,45 @@
             def _():
                 back_copy(j).wait_send()
                 tail_copy(j).wait_send()
-
-
-def delta(n, seqs, heads, rows4, small, par, gain, nq, nk, nv, nb, nd):
-    _, rows, width = rows4.shape
-    span, extent = rows // seqs, width // heads
+    for s in range(seqs):
+        for ck in range(chunks):
+            part_copy(s, ck).wait_send()
+            for d in range(1, chips):
+                cross_copy(d, s, ck).wait_send()
+                fwd_copy(d, s, ck).wait_send()
+
+
+def run(n, tp, tokens, weights, bw, dw, bias, rate, gain, nq, nk, nv, nb, nd):
+    seqs, span, kd = tokens.shape
+    heads, depth = bw.shape
+    width = weights[0].shape[1]
+    rows, extent = seqs * span, width // heads
     pairs = seqs * heads
+    chips = tp // 2
+    kc = 256 if kd % 256 == 0 else kd
+    chunks = kd // kc
     key_rows = extent // n
     tail = -(-key_rows // PAD) * PAD + PAD
     vmem = pl.BlockSpec(memory_space=pltpu.VMEM)
     smem = pl.BlockSpec(memory_space=pltpu.SMEM)
+    hbm = pl.BlockSpec(memory_space=pl.ANY)
     return pl.pallas_call(
-        functools.partial(delta_kernel, n, seqs, heads, 2),
+        functools.partial(kernel, n, tp, 2),
         out_shape=(
             jax.ShapeDtypeStruct((rows, width), bf16),
             jax.ShapeDtypeStruct((pairs, key_rows, extent), bf16),
             jax.ShapeDtypeStruct((pairs, extent), f32),
         ),
-        in_specs=[vmem] * 7 + [smem] * 2,
+        in_specs=[hbm] * 5 + [vmem] * 2 + [smem] * 2 + [vmem] * 4 + [smem] * 2,
         out_specs=(vmem,) * 3,
         scratch_shapes=[
+            pltpu.VMEM((seqs, span, kd), bf16),
+            pltpu.VMEM((tp, seqs, chunks, span, kc), bf16),
+            pltpu.VMEM((4, tp, kd, width), bf16),
+            pltpu.VMEM((4, rows, width), f32),
+            pltpu.VMEM((seqs, 2 * PAD, span), f32),
+            pltpu.VMEM((2 * PAD, depth), bf16),
+            pltpu.VMEM((4, rows, width), bf16),
             pltpu.VMEM((seqs, PAD, span), f32),
             pltpu.VMEM((seqs, span, PAD), f32),
             pltpu.VMEM((seqs, span, PAD), f32),
@@ -437,6 +432,12 @@
             pltpu.VMEM((pairs, extent, extent), bf16),
             pltpu.VMEM((n, tail, extent), f32),
             pltpu.VMEM((pairs, tail, extent), f32),
+            pltpu.SemaphoreType.DMA((seqs,)),
+            pltpu.SemaphoreType.DMA((4, tp)),
+            pltpu.SemaphoreType.DMA((chips - 1, seqs, chunks)),
+            pltpu.SemaphoreType.DMA((seqs, chunks)),
+            pltpu.SemaphoreType.DMA((chips - 1, seqs, chunks)),
+            pltpu.SemaphoreType.DMA((tp, seqs, chunks)),
             pltpu.SemaphoreType.DMA((pairs,)),
             pltpu.SemaphoreType.DMA((n,)),
             pltpu.SemaphoreType.DMA((n,)),
@@ -445,9 +446,9 @@
             pltpu.SemaphoreType.DMA((pairs,)),
         ],
         compiler_params=pltpu.CompilerParams(
-            collective_id=1, has_side_effects=True, vmem_limit_bytes=48 * 1024 * 1024
+            collective_id=0, has_side_effects=True, vmem_limit_bytes=56 * 1024 * 1024
         ),
-    )(rows4, small, par, gain, nq, nk, nv, nb, nd)
+    )(tokens, *weights, bw, dw, bias, rate, gain, nq, nk, nv, nb, nd)
 
 
 def shards(
@@ -458,16 +459,10 @@
     heads = rate_log.shape[0]
     extent = out_gain.shape[0]
     tp, sp = lax.axis_size("tp"), lax.axis_size("sp")
-    fill = ((0, PAD - heads), (0, 0))
-    bd = jnp.concatenate([jnp.pad(beta_weight.T, fill), jnp.pad(decay_weight.T, fill)], axis=0)
-    par = jnp.concatenate(
-        [jnp.pad(beta_bias[:, None], fill), jnp.pad(rate_log[:, None], fill)], axis=0
-    )
     weights = (query_weight, key_weight, value_weight, gate_weight)
-    rows4, small = gather_project(tp, seqs, tokens.reshape(seqs * span, kd), weights, bd)
-    mixed, cache, first = delta(
-        sp, seqs, heads, rows4, small, par, out_gain[None], new_query, new_key, new_value,
-        new_beta, new_decay,
+    mixed, cache, first = run(
+        sp, tp, tokens, weights, beta_weight.T, decay_weight.T, beta_bias, rate_log,
+        out_gain[None], new_query, new_key, new_value, new_beta, new_decay,
     )
     return (
         mixed.reshape(seqs, span, heads * extent),

time: 64.6 us -> 68.2 us (1.056)
  Pallas kernels: 56.8 us -> 62.8 us
  other arithmetic: 2.2 us -> 0 us
    pallas_call x2 -> x1, Pallas kernels: 56.8 us -> 62.8 us  [run(): pl.pallas_call(functools.partial(kernel, n, tp, 2), out_shape=(jax.ShapeD...]
    concatenate x2 -> x0, other arithmetic: 2.2 us -> none  [the longest x1 1.45 us: shards(): jnp.concatenate([jnp.pad(beta_weight.T, fill), jnp.pad(decay_weight.T, fi...]
    reshape x1, local copies, waits for them, and re-layouts: 0.6 us -> 1.28 us  [shards(): first.reshape(seqs, heads * extent)]
    unnamed x18 -> x2, local copies, waits for them, and re-layouts: 3.55 us -> 3.14 us
where the time goes in v2:
time: 68.2 us; the launch traced here: 67.9 us
  Pallas kernels  62.8 us (92%)
  local copies, waits for them, and re-layouts  4.42 us (6%)
    pallas_call x1, Pallas kernels, run(): pl.pallas_call(functools.partial(kernel, n, tp, 2), out_shape=(jax.ShapeD...  62.8 us
    unnamed x2, local copies, waits for them, and re-layouts  3.14 us

profile of v2, /device:TPU:0, one launch (start us, length us, event | category | flops | bytes accessed | tf_op | source)
XLA Modules:
  0.0 67.9 jit_solution(17624233112134430588)
XLA Ops:
  0.6 62.8 %shard_map.166 = (bf16[384,512]{1,0:T(8,128)(2,1)}, bf16[8,16,128]{2,1,0:T(8,128)(2,1)}, f32[8,128]{1,0:T(8,128)}) custom-call(bf16[2,192,1024]{2,1,0:T(8,128)(2,1)} %x_hbm.1, bf16[4096,512]{1,0:T(8,128)(2,1)} %wq_ref.1, bf16[4096,512]{1,0:T(8,128)(2,1)} %wk_ref.1, bf16[4096,512]{1,0:T(8,128)(2,1)} %wv_ref.1, bf16[4096,512]{1,0:T(8,128)(2,1)} %wg_ref.1, ...), custom_call_target="tpu_custom_call" | custom-call | tf_op jit(solution)/shard_map/pallas_call | solution.py:407
  63.5 1.3 %reshape.17 = f32[2,512]{1,0:T(2,128)} reshape(f32[8,128]{1,0:T(8,128)} %get-tuple-element.8) | data formatting | bytes 8192 | tf_op jit(solution)/shard_map/reshape | solution.py:470
  64.7 1.8 %copy.20 = bf16[2,192,512]{2,1,0:T(8,128)(2,1)} copy(bf16[2,192,512]{2,1,0:T(8,128)(2,1)} %bitcast.5) | data formatting | bytes 786432
  66.5 1.4 %copy.21 = bf16[2,4,16,128]{3,2,1,0:T(8,128)(2,1)} copy(bf16[2,4,16,128]{3,2,1,0:T(8,128)(2,1)} %bitcast.8) | data formatting | bytes 65536

commit v3 on v1

--- a/solution.py
+++ b/solution.py
@@ -25,8 +25,8 @@
 
 
 def gather_kernel(
-    n, seqs, x_ref, wq_ref, wk_ref, wv_ref, wg_ref, bd_ref, out_ref, small_ref,
-    xs, wbuf, acc, sacc, wsem, cross_sem, part_sem, fwd_sem, rx,
+    n, seqs, x_ref, wq_ref, wk_ref, wv_ref, wg_ref, bw_ref, dw_ref, out_ref,
+    small_ref, bd_ref, xs, wbuf, acc, sacc, wsem, cross_sem, part_sem, fwd_sem, rx,
 ):
     me = lax.axis_index("tp")
     y, c = me // 2, lax.rem(me, 2)
@@ -57,6 +57,9 @@
     for slot in range(n):
         for w in range(4):
             weight_copy(w, slot).start()
+    bd_ref[...] = jnp.zeros_like(bd_ref)
+    bd_ref[0 : bw_ref.shape[0]] = bw_ref[...]
+    bd_ref[PAD : PAD + dw_ref.shape[0]] = dw_ref[...]
     pl.semaphore_wait(barrier, chips)
 
     def cols(ck):
@@ -138,7 +141,7 @@
             fwd_copy(d, ck).wait_send()
 
 
-def gather_project(n, seqs, tokens, weights, bd):
+def gather_project(n, seqs, tokens, weights, bw, dw):
     rows, kd = tokens.shape
     width = weights[0].shape[1]
     kc = 256 if kd % 256 == 0 else kd
@@ -153,9 +156,10 @@
         ),
         in_specs=[pl.BlockSpec(memory_space=pltpu.VMEM)]
         + [pl.BlockSpec(memory_space=pl.ANY)] * 4
-        + [pl.BlockSpec(memory_space=pltpu.VMEM)],
+        + [pl.BlockSpec(memory_space=pltpu.VMEM)] * 2,
         out_specs=(pl.BlockSpec(memory_space=pltpu.VMEM),) * 2,
         scratch_shapes=[
+            pltpu.VMEM((2 * PAD, bw.shape[1]), bf16),
             pltpu.VMEM((n, chunks, rows, kc), bf16),
             pltpu.VMEM((4, n, kd, width), bf16),
             pltpu.VMEM((4, rows, width), f32),
@@ -169,7 +173,7 @@
         compiler_params=pltpu.CompilerParams(
             collective_id=0, has_side_effects=True, vmem_limit_bytes=60 * 1024 * 1024
         ),
-    )(tokens, *weights, bd)
+    )(tokens, *weights, bw, dw)
 
 
 def unit_rows(values):
@@ -177,7 +181,7 @@
 
 
 def delta_kernel(
-    n, seqs, heads, group, rows_ref, small_ref, par_ref, gain_ref, nq_ref, nk_ref, nv_ref,
+    n, seqs, heads, group, rows_ref, small_ref, bias_ref, rate_ref, gain_ref, nq_ref, nk_ref, nv_ref,
     nb_ref, nd_ref, mixed_ref, cache_ref, first_ref,
     cum_row, cum_col, beta_col, local_out, reach, out_box, in_box, back_out, back_in, tail_out,
     tail_in, send1, recv1, send2, recv2, send3, recv3,
@@ -196,7 +200,12 @@
     row = lax.broadcasted_iota(jnp.int32, (span, span), 0)
     col = lax.broadcasted_iota(jnp.int32, (span, span), 1)
     upper = jnp.where(row <= col, 1.0, 0.0)
-    bias, rate = par_ref[0:PAD], par_ref[PAD : 2 * PAD]
+    slot_of = lax.broadcasted_iota(jnp.int32, (PAD, 1), 0)
+    bias = jnp.zeros((PAD, 1), f32)
+    rate = jnp.zeros((PAD, 1), f32)
+    for h in range(heads):
+        bias = jnp.where(slot_of == h, bias_ref[h], bias)
+        rate = jnp.where(slot_of == h, rate_ref[h], rate)
     for s in range(seqs):
         beta = jax.nn.sigmoid(small_ref[s, 0:PAD, :] + bias)
         pre = small_ref[s, PAD : 2 * PAD, :]
@@ -408,7 +417,7 @@
                 tail_copy(j).wait_send()
 
 
-def delta(n, seqs, heads, rows4, small, par, gain, nq, nk, nv, nb, nd):
+def delta(n, seqs, heads, rows4, small, bias, rate, gain, nq, nk, nv, nb, nd):
     _, rows, width = rows4.shape
     span, extent = rows // seqs, width // heads
     pairs = seqs * heads
@@ -423,7 +432,7 @@
             jax.ShapeDtypeStruct((pairs, key_rows, extent), bf16),
             jax.ShapeDtypeStruct((pairs, extent), f32),
         ),
-        in_specs=[vmem] * 7 + [smem] * 2,
+        in_specs=[vmem] * 2 + [smem] * 2 + [vmem] * 4 + [smem] * 2,
         out_specs=(vmem,) * 3,
         scratch_shapes=[
             pltpu.VMEM((seqs, PAD, span), f32),
@@ -447,7 +456,7 @@
         compiler_params=pltpu.CompilerParams(
             collective_id=1, has_side_effects=True, vmem_limit_bytes=48 * 1024 * 1024
         ),
-    )(rows4, small, par, gain, nq, nk, nv, nb, nd)
+    )(rows4, small, bias, rate, gain, nq, nk, nv, nb, nd)
 
 
 def shards(
@@ -458,15 +467,10 @@
     heads = rate_log.shape[0]
     extent = out_gain.shape[0]
     tp, sp = lax.axis_size("tp"), lax.axis_size("sp")
-    fill = ((0, PAD - heads), (0, 0))
-    bd = jnp.concatenate([jnp.pad(beta_weight.T, fill), jnp.pad(decay_weight.T, fill)], axis=0)
-    par = jnp.concatenate(
-        [jnp.pad(beta_bias[:, None], fill), jnp.pad(rate_log[:, None], fill)], axis=0
-    )
     weights = (query_weight, key_weight, value_weight, gate_weight)
-    rows4, small = gather_project(tp, seqs, tokens.reshape(seqs * span, kd), weights, bd)
+    rows4, small = gather_project(tp, seqs, tokens.reshape(seqs * span, kd), weights, beta_weight.T, decay_weight.T)
     mixed, cache, first = delta(
-        sp, seqs, heads, rows4, small, par, out_gain[None], new_query, new_key, new_value,
+        sp, seqs, heads, rows4, small, beta_bias, rate_log, out_gain[None], new_query, new_key, new_value,
         new_beta, new_decay,
     )
     return (

time: 64.6 us -> 62.3 us (0.964)
  other arithmetic: 2.2 us -> 0 us
    concatenate x2 -> x0, other arithmetic: 2.2 us -> none  [the longest x1 1.45 us: shards(): jnp.concatenate([jnp.pad(beta_weight.T, fill), jnp.pad(decay_weight.T, fi...]
    unnamed x18 -> x22, local copies, waits for them, and re-layouts: 3.55 us -> 3.55 us
where the time goes in v3:
time: 62.3 us; the launch traced here: 61.7 us
  Pallas kernels  56.8 us (91%)
  local copies, waits for them, and re-layouts  4.15 us (7%)
  between operations  0.79 us (1%)
    pallas_call x1, Pallas kernels, delta(): pl.pallas_call(functools.partial(delta_kernel, n, seqs, heads, 2), out_sh...  31 us
    pallas_call x1, Pallas kernels, gather_project(): pl.pallas_call(functools.partial(gather_kernel, n, seqs), out_shape=(jax....  25.8 us
    unnamed x22, local copies, waits for them, and re-layouts  3.55 us

profile of v3, /device:TPU:0, one launch (start us, length us, event | category | flops | bytes accessed | tf_op | source)
XLA Modules:
  0.0 61.7 jit_solution(6960686819547109848)
XLA Ops:
  0.6 0.0 copy-start.2
  0.6 0.0 copy-start.3
  0.7 0.0 copy-start.4
  0.7 0.0 copy-start.5
  0.7 0.0 copy-start.6
  0.7 0.0 copy-start.7
  0.7 0.0 copy-start.8
  0.7 0.0 copy-start.9
  0.7 25.8 %shard_map.166 = (bf16[4,384,512]{2,1,0:T(8,128)(2,1)}, f32[2,16,192]{2,1,0:T(8,128)}) custom-call(bf16[384,1024]{1,0:T(8,128)(2,1)} %bitcast.9, bf16[4096,512]{1,0:T(8,128)(2,1)} %wq_ref.1, bf16[4096,512]{1,0:T(8,128)(2,1)} %wk_ref.1, bf16[4096,512]{1,0:T(8,128)(2,1)} %wv_ref.1, bf16[4096,512]{1,0:T(8,128)(2,1)} %wg_ref.1, bf16[4,4096]{1,0:T(4,128)(2,1)} %bitcast.10, ...), custom_call_target="tpu_custom_call" | custom-call | tf_op jit(solution)/shard_map/pallas_call | solution.py:151
  26.5 0.0 copy-done.2
  26.5 0.0 copy-done.3
  26.6 0.0 copy-done.4
  26.6 0.0 copy-done.5
  26.6 0.0 copy-done.6
  26.6 0.0 copy-done.7
  26.6 0.0 copy-done.8
  26.6 0.0 copy-done.9
  26.6 0.0 copy-start
  26.6 1.4 %copy-done = bf16[4,384,512]{2,1,0:T(8,128)(2,1)S(1)} copy-done((bf16[4,384,512]{2,1,0:T(8,128)(2,1)S(1)}, bf16[4,384,512]{2,1,0:T(8,128)(2,1)}, u32[]{:S(2)}) %copy-start) | copy-done | bytes 1572888
  28.0 0.8 %copy-done.1 = f32[2,16,192]{2,1,0:T(8,128)S(1)} copy-done((f32[2,16,192]{2,1,0:T(8,128)S(1)}, f32[2,16,192]{2,1,0:T(8,128)}, u32[]{:S(2)}) %copy-start.1) | copy-done | bytes 24600
  28.8 31.0 %shard_map.167 = (bf16[384,512]{1,0:T(8,128)(2,1)S(1)}, bf16[8,16,128]{2,1,0:T(8,128)(2,1)S(1)}, f32[8,128]{1,0:T(8,128)S(1)}) custom-call(bf16[4,384,512]{2,1,0:T(8,128)(2,1)S(1)} %copy-done, f32[2,16,192]{2,1,0:T(8,128)S(1)} %copy-done.1, f32[4]{0:T(128)S(1)} %copy-done.7, f32[4]{0:T(128)S(1)} %copy-done.8, f32[1,128]{1,0:T(1,128)S(1)} %bitcast.8, ...), custom_call_target="tpu_custom_call" | custom-call | tf_op jit(solution)/shard_map/pallas_call | solution.py:428
  59.8 0.6 reshape.21
  60.4 0.7 %copy.20 = bf16[2,192,512]{2,1,0:T(8,128)(2,1)} copy(bf16[2,192,512]{2,1,0:T(8,128)(2,1)S(1)} %bitcast.6) | data formatting | bytes 786432
  61.1 0.6 copy.21
  (1 shorter events, 0.0 us)
Async XLA Ops:
  0.6 25.9 %copy-start.2 = (bf16[2,4,128]{2,1,0:T(4,128)(2,1)S(1)}, bf16[2,4,128]{2,1,0:T(4,128)(2,1)}, u32[]{:S(2)}) copy-start(bf16[2,4,128]{2,1,0:T(4,128)(2,1)} %nq_ref.1) | copy-start | bytes 6148
  0.6 25.9 %copy-start.3 = (bf16[2,4,128]{2,1,0:T(4,128)(2,1)S(1)}, bf16[2,4,128]{2,1,0:T(4,128)(2,1)}, u32[]{:S(2)}) copy-start(bf16[2,4,128]{2,1,0:T(4,128)(2,1)} %nk_ref.1) | copy-start | bytes 6148
  0.7 25.9 %copy-start.4 = (bf16[2,4,128]{2,1,0:T(4,128)(2,1)S(1)}, bf16[2,4,128]{2,1,0:T(4,128)(2,1)}, u32[]{:S(2)}) copy-start(bf16[2,4,128]{2,1,0:T(4,128)(2,1)} %nv_ref.1) | copy-start | bytes 6148
  0.7 25.9 %copy-start.5 = (f32[2,4]{1,0:T(2,128)S(1)}, f32[2,4]{1,0:T(2,128)}, u32[]{:S(2)}) copy-start(f32[2,4]{1,0:T(2,128)} %nb_ref.1) | copy-start | bytes 100
  0.7 25.9 %copy-start.6 = (f32[2,4]{1,0:T(2,128)S(1)}, f32[2,4]{1,0:T(2,128)}, u32[]{:S(2)}) copy-start(f32[2,4]{1,0:T(2,128)} %nd_ref.1) | copy-start | bytes 100
  0.7 25.9 %copy-start.7 = (f32[4]{0:T(128)S(1)}, f32[4]{0:T(128)}, u32[]{:S(2)}) copy-start(f32[4]{0:T(128)} %bias_ref.1) | copy-start | bytes 52
  0.7 25.9 %copy-start.8 = (f32[4]{0:T(128)S(1)}, f32[4]{0:T(128)}, u32[]{:S(2)}) copy-start(f32[4]{0:T(128)} %rate_ref.1) | copy-start | bytes 52
  0.7 25.9 %copy-start.9 = (f32[128]{0:T(128)S(1)}, f32[128]{0:T(128)}, u32[]{:S(2)}) copy-start(f32[128]{0:T(128)} %param.24) | copy-start | bytes 1540
  26.6 1.4 %copy-start = (bf16[4,384,512]{2,1,0:T(8,128)(2,1)S(1)}, bf16[4,384,512]{2,1,0:T(8,128)(2,1)}, u32[]{:S(2)}) copy-start(bf16[4,384,512]{2,1,0:T(8,128)(2,1)} %get-tuple-element.8.rows_ref) | copy-start | bytes 4718596
  28.0 0.8 %copy-start.1 = (f32[2,16,192]{2,1,0:T(8,128)S(1)}, f32[2,16,192]{2,1,0:T(8,128)}, u32[]{:S(2)}) copy-start(f32[2,16,192]{2,1,0:T(8,128)} %get-tuple-element.9.small_ref) | copy-start | bytes 73732
